TPU v7x, 32 devices: a whole 2x2x4 slice. The times are simulated.
32 devices in a mesh: sp: 8 (over z, x), tp: 4 (over y, core).
Axes of the slice: x: 2, y: 2, z: 4, core: 2. Of those that a mesh axis runs over, the one named last changes fastest.
Arguments:
- result_cotangent_values: bfloat16 [1024, 2048], P('sp'), may hold values from -6 to 6
- specialist_entry_vectors: bfloat16 [1024, 2048], P('sp'), may hold values from -6 to 6
- chosen_specialists: int32 [1024, 2], P('sp'), may hold values from 0 to 3, all different within a row; in each aligned block of 128 rows (0 to 127, 128 to 255, ...) at most 128 rows name the same one
- specialist_mixing_shares: float32 [1024, 2], P('sp'), may hold values from 0.1 to 0.9
- specialist_switch_maps: bfloat16 [8, 2048, 1792], P('sp', None, 'tp'), may hold values from -0.125 to 0.125
- specialist_widen_maps: bfloat16 [8, 2048, 1792], P('sp', None, 'tp'), may hold values from -0.125 to 0.125
- specialist_shrink_maps: bfloat16 [8, 1792, 2048], P('sp', 'tp'), may hold values from -0.09375 to 0.09375
- memory_readout_map: bfloat16 [2048, 2048], P('sp', 'tp'), may hold values from -0.125 to 0.125
- memory_source_vectors: bfloat16 [1024, 2048], P('sp', 'tp'), may hold values from -6 to 6
- memory_hidden_values: bfloat16 [1024, 2048], P('sp', 'tp'), may hold values from -6 to 6
- feature_fading_speed: float32 [2048], P('tp'), may hold values from 1.6276042e-05 to 0.009
- extra_log_fading: float32 [1024], P('sp'), may hold values from -2.8 to 0
- memory_switch_tiles: bfloat16 [8, 256, 256], P('tp'), may hold values from -0.375 to 0.375
- entry_switch_tiles: bfloat16 [8, 256, 256], P('tp'), may hold values from -0.375 to 0.375
Outputs:
- gate_proj_grad: bfloat16 [8, 2048, 1792], P('sp', None, 'tp')
- up_proj_grad: bfloat16 [8, 2048, 1792], P('sp', None, 'tp')
- down_proj_grad: bfloat16 [8, 1792, 2048], P('sp', 'tp')
- out_proj_grad: float32 [2048, 2048], P('sp', 'tp')
- lru_input_grad: float32 [1024, 2048], P('sp', 'tp')
Inputs may be any that keep to these rules, and one draw needn't show every extreme that they name: `chosen_specialists`: each token names two different experts; among the 128 tokens of one device no expert is named more than 128 times, a bound that some block reaches on some device.
All inputs are finite; a program needn't handle non-finite values.
Results may differ from a plain program's by a relative error of at most 0.009.
Values may be sent and summed in bfloat16 or wider, within the bound.
A program may use at most 128 MiB of HBM per device.

v0:
```python
import jax
import jax.numpy as jnp
from jax import lax
from jax.sharding import PartitionSpec as P

SLICES = 2


def prefix(part, axis, combine, identity):
    count = lax.axis_size(axis)
    place = lax.axis_index(axis)
    ahead = count - 1 - place
    gathered = jax.tree.map(lambda a: lax.all_gather(a, axis), part)
    state = jax.tree.map(lambda a, e: jnp.zeros_like(a) + jnp.asarray(e, a.dtype), part, identity)

    def one(turn, state):
        source = count - 1 - turn
        return combine(
            state, jax.tree.map(lambda a: lax.dynamic_index_in_dim(a, source, 0, False), gathered)
        )

    return lax.fori_loop(0, ahead, one, state)


def silu_slope(value):
    sig_value = jax.nn.sigmoid(value)
    return sig_value * (1.0 + value * (1.0 - sig_value))


def compose(upper_map, lower_map):
    return (lower_map[0] * upper_map[0], lower_map[1] + lower_map[0] * upper_map[1])


def chain_join(higher_map, lower_map):
    return (lower_map[0] * higher_map[0], lower_map[1] + lower_map[0] * higher_map[1])


def expert_backward(inputs, grads_in, gate_weight, up_weight, down_weight):
    gate_value = jnp.dot(inputs, gate_weight, preferred_element_type=jnp.float32)
    up_value = jnp.dot(inputs, up_weight, preferred_element_type=jnp.float32)
    active = jax.nn.silu(gate_value)
    hidden = (active * up_value).astype(jnp.bfloat16)
    down_grad = jnp.einsum(
        "rf,rd->fd", hidden, grads_in, preferred_element_type=jnp.float32
    ).astype(jnp.bfloat16)
    hidden_grad = jnp.einsum("rd,fd->rf", grads_in, down_weight, preferred_element_type=jnp.float32)
    gate_grad = (hidden_grad * up_value * silu_slope(gate_value)).astype(jnp.bfloat16)
    up_grad = (hidden_grad * active).astype(jnp.bfloat16)
    gate_weight_grad = jnp.einsum(
        "rd,rf->df", inputs, gate_grad, preferred_element_type=jnp.float32
    ).astype(jnp.bfloat16)
    up_weight_grad = jnp.einsum(
        "rd,rf->df", inputs, up_grad, preferred_element_type=jnp.float32
    ).astype(jnp.bfloat16)
    token_part = jnp.einsum("rf,df->rd", gate_grad, gate_weight, preferred_element_type=jnp.float32)
    token_part = token_part + jnp.einsum(
        "rf,df->rd", up_grad, up_weight, preferred_element_type=jnp.float32
    )
    return (gate_weight_grad, up_weight_grad, down_grad, token_part)


def collect(returned, targets, route_count):
    gathered = jnp.take(returned, targets[0], axis=0).astype(jnp.float32)
    for target in targets[1:]:
        gathered = gathered + jnp.take(returned, target, axis=0).astype(jnp.float32)
    return gathered.reshape(-1, route_count, gathered.shape[-1]).sum(axis=1)


def fill_slots(values, targets, slot_rows):
    buffer = jnp.zeros((slot_rows, values.shape[1]), jnp.bfloat16)
    for target in targets:
        buffer = buffer.at[target].set(values)
    return buffer


def local(
    result_cotangent_values,
    specialist_entry_vectors,
    chosen_specialists,
    specialist_mixing_shares,
    specialist_switch_maps,
    specialist_widen_maps,
    specialist_shrink_maps,
    memory_readout_map,
    memory_source_vectors,
    memory_hidden_values,
    feature_fading_speed,
    extra_log_fading,
    memory_switch_tiles,
    entry_switch_tiles,
):
    tok_rows, feature_count = result_cotangent_values.shape
    route_count = chosen_specialists.shape[1]
    sp_count = lax.axis_size("sp")
    expert_count = sp_count // SLICES
    capacity = min(tok_rows, 4 * tok_rows // expert_count)
    slot_rows = sp_count * capacity
    flat_expert = chosen_specialists.reshape(-1)
    onehot = (flat_expert[:, None] == jnp.arange(expert_count, dtype=jnp.int32)[None, :]).astype(
        jnp.int32
    )
    slot_rank = jnp.sum((jnp.cumsum(onehot, axis=0) - 1) * onehot, axis=1)
    scaled = (
        (
            specialist_mixing_shares[:, :, None]
            * result_cotangent_values[:, None, :].astype(jnp.float32)
        )
        .astype(jnp.bfloat16)
        .reshape(-1, feature_count)
    )
    copies = jnp.broadcast_to(
        specialist_entry_vectors[:, None, :], (tok_rows, route_count, feature_count)
    ).reshape(-1, feature_count)
    targets = [
        (flat_expert * SLICES + slice_index) * capacity + slot_rank for slice_index in range(SLICES)
    ]
    share = feature_count // lax.axis_size("tp")
    first_col = lax.axis_index("tp") * share
    part_grad = lax.dynamic_slice_in_dim(scaled, first_col, share, 1)
    part_rows = lax.dynamic_slice_in_dim(copies, first_col, share, 1)
    send_grad = fill_slots(part_grad, targets, slot_rows)
    send_rows = fill_slots(part_rows, targets, slot_rows)
    got_grad, got_rows = (
        lax.all_to_all(
            send_grad.reshape(sp_count, capacity, share),
            "sp",
            split_axis=0,
            concat_axis=0,
            tiled=True,
        ),
        lax.all_to_all(
            send_rows.reshape(sp_count, capacity, share),
            "sp",
            split_axis=0,
            concat_axis=0,
            tiled=True,
        ),
    )
    recv_grad, recv_rows = (
        lax.all_gather(got_grad, "tp", axis=2, tiled=True),
        lax.all_gather(got_rows, "tp", axis=2, tiled=True),
    )
    inputs = recv_rows.reshape(slot_rows, feature_count)
    grads_in = recv_grad.reshape(slot_rows, feature_count)
    gate_weight_grad, up_weight_grad, down_grad, token_part = expert_backward(
        inputs,
        grads_in,
        specialist_switch_maps[0],
        specialist_widen_maps[0],
        specialist_shrink_maps[0],
    )
    returned = lax.all_to_all(
        token_part.astype(jnp.bfloat16).reshape(sp_count, capacity, feature_count),
        "sp",
        split_axis=0,
        concat_axis=0,
        tiled=True,
    )
    own_sum = collect(returned.reshape(slot_rows, feature_count), targets, route_count)
    moe_grad = lax.psum(own_sum.astype(jnp.bfloat16), "tp").astype(jnp.float32)
    mixed_grad = (result_cotangent_values.astype(jnp.float32) + moe_grad).astype(jnp.bfloat16)
    col_count = memory_readout_map.shape[1]
    columns = mixed_grad
    upstream = jnp.dot(
        columns,
        lax.all_gather(memory_readout_map, "sp", axis=0, tiled=True),
        preferred_element_type=jnp.float32,
    )
    blocks_here = memory_switch_tiles.shape[0]
    block_width = memory_switch_tiles.shape[1]
    blocks_in = memory_source_vectors.reshape(tok_rows, blocks_here, block_width)
    memory_switch_fraction = jax.nn.sigmoid(
        jnp.einsum(
            "tnc,ncd->tnd", blocks_in, memory_switch_tiles, preferred_element_type=jnp.float32
        ).reshape(tok_rows, col_count)
    )
    inp_open = jax.nn.sigmoid(
        jnp.einsum(
            "tnc,ncd->tnd", blocks_in, entry_switch_tiles, preferred_element_type=jnp.float32
        ).reshape(tok_rows, col_count)
    )
    xin = memory_source_vectors.astype(jnp.float32)
    log_fading_factor = (
        -8.0 * memory_switch_fraction * feature_fading_speed[None, :] + extra_log_fading[:, None]
    )
    decay_mult = jnp.exp(log_fading_factor)
    spare_room = -jnp.expm1(2.0 * log_fading_factor)
    in_scale = jnp.sqrt(jnp.maximum(spare_room, 0.01))
    drive = in_scale * inp_open * xin
    coeff = jnp.concatenate([decay_mult[1:], jnp.ones((1, col_count), jnp.float32)], axis=0)
    prod_after, local_part = lax.associative_scan(compose, (coeff, upstream), reverse=True, axis=0)
    alpha_part = decay_mult[0] * local_part[0]
    beta_part = decay_mult[0] * prod_after[0]
    carried = prefix(
        (beta_part, alpha_part),
        "sp",
        chain_join,
        (jnp.ones_like(beta_part), jnp.zeros_like(alpha_part)),
    )
    incoming = carried[1]
    dstate = local_part + prod_after * incoming[None, :]
    scale_slope = jnp.where(spare_room > 0.01, -decay_mult * decay_mult / in_scale, 0.0)
    log_grad = dstate * (
        memory_hidden_values.astype(jnp.float32) - drive + scale_slope * inp_open * xin
    )
    grad_rec = (
        log_grad
        * (-8.0 * feature_fading_speed[None, :])
        * memory_switch_fraction
        * (1.0 - memory_switch_fraction)
    ).astype(jnp.bfloat16)
    grad_in = (dstate * in_scale * xin * inp_open * (1.0 - inp_open)).astype(jnp.bfloat16)
    back_rec = jnp.einsum(
        "tnd,ncd->tnc",
        grad_rec.reshape(tok_rows, blocks_here, block_width),
        memory_switch_tiles,
        preferred_element_type=jnp.float32,
    )
    back_in = jnp.einsum(
        "tnd,ncd->tnc",
        grad_in.reshape(tok_rows, blocks_here, block_width),
        entry_switch_tiles,
        preferred_element_type=jnp.float32,
    )
    lru_input_grad = (
        dstate * in_scale * inp_open
        + back_rec.reshape(tok_rows, col_count)
        + back_in.reshape(tok_rows, col_count)
    )
    columns = mixed_grad
    out_proj_grad = lax.psum_scatter(
        jnp.einsum("tr,tc->rc", columns, memory_hidden_values, preferred_element_type=jnp.float32),
        "sp",
        scatter_dimension=0,
        tiled=True,
    )
    return (
        gate_weight_grad[None],
        up_weight_grad[None],
        down_grad[None],
        out_proj_grad,
        lru_input_grad,
    )


def solution(mesh):
    return jax.shard_map(
        local,
        mesh=mesh,
        in_specs=(
            P("sp", None),
            P("sp", None),
            P("sp", None),
            P("sp", None),
            P("sp", None, "tp"),
            P("sp", None, "tp"),
            P("sp", "tp", None),
            P("sp", "tp"),
            P("sp", "tp"),
            P("sp", "tp"),
            P("tp"),
            P("sp"),
            P("tp", None, None),
            P("tp", None, None),
        ),
        out_specs=(
            P("sp", None, "tp"),
            P("sp", None, "tp"),
            P("sp", "tp", None),
            P("sp", "tp"),
            P("sp", "tp"),
        ),
        check_vma=False,
    )
```

profile of v0, /device:TPU:0, one launch (start us, length us, event | category | flops | bytes accessed | tf_op | source)
XLA Modules:
  0.0 415.5 jit_solution(13920813753677419819)
XLA Ops:
  8.1 0.8 add_multiply_fusion.12
  8.9 0.8 copy.49
  9.7 0.1 eq.29
  9.8 0.1 eq.25
  9.9 0.1 copy.53
  10.1 0.1 mul.272
  10.2 1.2 reduce-window.6
  11.9 0.1 mul.267
  12.1 1.7 broadcast_in_dim.22
  13.8 1.2 reshape.168
  15.0 3.0 scatter_custom_fusion
  18.0 4.2 %scatter_custom_fusion.1 = bf16[1024,512]{1,0:T(8,128)(2,1)} fusion(bf16[1024,512]{1,0:T(8,128)(2,1)} %scatter_custom_fusion, s32[256]{0:T(256)S(1)} %bitcast.121, bf16[256,2048]{1,0:T(8,128)(2,1)} %reshape.168, s32[]{:T(128)} %constant.77.clone.1, s32[]{:T(128)S(6)} %select_n.47), kind=kCustom, calls=%fused_computation.72 | custom fusion | bytes 1311236 | tf_op jit(solution)/shard_map/scatter | solution.py:72
  22.3 33.3 %all_to_all.15 = bf16[8,128,512]{2,1,0:T(8,128)(2,1)} all-to-all(bf16[8,128,512]{2,1,0:T(8,128)(2,1)} %bitcast.7), channel_id=1, replica_groups=mesh['sp'=8,'tp'=4] {'sp'}, dimensions={0} | all-to-all | bytes 2097152 | tf_op jit(solution)/shard_map/all_to_all | solution.py:131
  55.6 2.4 mul.275
  58.1 3.8 mul.276
  61.8 0.1 copy.54
  62.0 0.1 mul.273
  62.1 3.3 scatter_custom_fusion.2
  65.4 4.4 %scatter_custom_fusion.3 = bf16[1024,512]{1,0:T(8,128)(2,1)} fusion(bf16[1024,512]{1,0:T(8,128)(2,1)} %scatter_custom_fusion.2, s32[256]{0:T(256)S(1)} %bitcast.122, f32[256,2048]{1,0:T(8,128)} %mul.276, s32[]{:T(128)S(6)} %select_n.47, f32[256]{0:T(256)S(1)} %mul.273), kind=kCustom, calls=%fused_computation.154 | custom fusion | flops 262144 | bytes 1573892 | tf_op jit(solution)/shard_map/scatter | solution.py:72
  69.8 29.4 %all_to_all.16 = bf16[8,128,512]{2,1,0:T(8,128)(2,1)} all-to-all(bf16[8,128,512]{2,1,0:T(8,128)(2,1)} %bitcast.106), channel_id=1, replica_groups=mesh['sp'=8,'tp'=4] {'sp'}, dimensions={0} | all-to-all | bytes 2097152 | tf_op jit(solution)/shard_map/all_to_all | solution.py:124
  99.2 5.7 %fusion.5 = f32[1024,448]{0,1:T(8,128)} fusion(bf16[1024,2048]{1,0:T(8,128)(2,1)} %bitcast.125, bf16[1,2048,448]{1,2,0:T(8,128)(2,1)S(1)} %copy-done), kind=kOutput, calls=%fused_computation.19 | convolution fusion | flops 1879048192 | bytes 7864320 | tf_op jit(solution)/shard_map/dot_general | solution.py:39
  104.9 3.4 fusion.8
  108.3 24.5 %all-gather.8.cloned.1.call-done = bf16[8,128,2048]{2,1,0:T(8,128)(2,1)} async-done(((bf16[8,128,512]{2,1,0:T(8,128)(2,1)}), bf16[8,128,2048]{2,1,0:T(8,128)(2,1)}) %all-gather.8.cloned.1.call-update) | async-done | bytes 4194320 | tf_op jit(solution)/shard_map/all_gather | solution.py:140
  132.8 6.4 %multiply_convert_fusion.1 = (bf16[1024,448]{0,1:T(8,128)(2,1)S(1)}, bf16[1024,448]{0,1:T(8,128)(2,1)S(1)}) fusion(f32[1024,448]{0,1:T(8,128)} %fusion.5, f32[1024,448]{0,1:T(8,128)} %fusion.8, bf16[1024,2048]{1,0:T(8,128)(2,1)} %bitcast.129, bf16[1,448,2048]{2,1,0:T(8,128)(2,1)} %param.24), kind=kOutput, calls=%fused_computation.27 | convolution fusion | flops 1885011968 | bytes 11534336 | tf_op jit(solution)/shard_map/rd,fd->rf/dot_general | solution.py:46
  139.2 2.4 fusion.3
  141.7 4.5 %add_convert_fusion = bf16[1024,2048]{1,0:T(8,128)(2,1)} fusion(f32[1024,2048]{1,0:T(8,128)S(1)} %fusion.3, bf16[1024,448]{0,1:T(8,128)(2,1)S(1)} %get-tuple-element.109, bf16[1,2048,448]{1,2,0:T(8,128)(2,1)S(1)} %copy-done.15), kind=kOutput, calls=%fused_computation.9 | convolution fusion | flops 1883242496 | bytes 15335424 | tf_op jit(solution)/shard_map/rf,df->rd/dot_general | solution.py:56
  146.2 5.5 %all-to-all-start.2 = ((bf16[8,128,2048]{2,1,0:T(8,128)(2,1)}), bf16[8,128,2048]{2,1,0:T(8,128)(2,1)}, u32[]{:S(2)}, u32[]{:S(2)}) async-start(bf16[8,128,2048]{2,1,0:T(8,128)(2,1)} %bitcast.105), calls=%async_computation.2 | async-start | bytes 8388608 | tf_op jit(solution)/shard_map/all_to_all | solution.py:152
  151.7 0.2 all-reduce.32.cloned.1.call-start
  152.0 93.4 %all-to-all-done.2 = bf16[8,128,2048]{2,1,0:T(8,128)(2,1)} async-done(((bf16[8,128,2048]{2,1,0:T(8,128)(2,1)}), bf16[8,128,2048]{2,1,0:T(8,128)(2,1)}, u32[]{:S(2)}, u32[]{:S(2)}) %all-to-all-start.2) | async-done | bytes 4194336 | tf_op jit(solution)/shard_map/all_to_all | solution.py:152
  245.4 6.1 %gather_fusion.1 = bf16[256,2048]{1,0:T(8,128)(2,1)} fusion(bf16[1024,2048]{1,0:T(8,128)(2,1)} %bitcast.18, s32[1024]{0:T(1024)S(1)} %get-tuple-element.150), kind=kCustom, calls=%fused_computation.1.clone | custom fusion | bytes 2098176 | tf_op jit(solution)/shard_map/jit(_take)/gather | solution.py:65
  251.4 6.1 %gather_fusion = bf16[256,2048]{1,0:T(8,128)(2,1)} fusion(bf16[1024,2048]{1,0:T(8,128)(2,1)} %bitcast.18, s32[1024]{0:T(1024)S(1)} %get-tuple-element.151), kind=kCustom, calls=%fused_computation.clone | custom fusion | bytes 2098176 | tf_op jit(solution)/shard_map/jit(_take)/gather | solution.py:63
  257.5 1.9 convert_add_fusion
  259.5 2.3 reshape.175
  261.7 5.0 %reduce_sum.22 = bf16[128,2048]{1,0:T(8,128)(2,1)} reduce(f32[128,2,2048]{2,1,0:T(2,128)} %reshape.175, f32[]{:T(128)} %constant.87.clone.1), dimensions={1}, to_apply=%region_7.9 | reduce | flops 262144 | bytes 2621444 | tf_op jit(solution)/shard_map/reduce_sum | solution.py:66
  266.8 0.5 all-gather.10.cloned.1.call-update
  267.4 0.3 reduce-scatter.2.cloned.1.call-start
  267.7 0.3 fusion.18
  268.0 0.1 copy.67
  268.7 0.3 fusion.15
  269.0 0.1 copy.68
  269.1 0.2 slice.246
  269.3 0.1 slice.250
  269.4 0.1 slice.256
  269.6 5.9 %fusion.1 = bf16[1,2048,448]{1,2,0:T(8,128)(2,1)} fusion(bf16[1024,448]{0,1:T(8,128)(2,1)} %copy-done.16, bf16[1024,2048]{1,0:T(8,128)(2,1)} %bitcast.126), kind=kOutput, calls=%fused_computation.14 | convolution fusion | flops 1879965696 | bytes 6946816 | tf_op jit(solution)/shard_map/rd,rf->df/dot_general | solution.py:49
  275.4 23.1 %all-reduce.32.cloned.1.call-done = bf16[128,2048]{1,0:T(8,128)(2,1)} async-done(((bf16[128,2048]{1,0:T(8,128)(2,1)}), bf16[128,2048]{1,0:T(8,128)(2,1)}) %all-reduce.32.cloned.1.call-update) | async-done | bytes 524304 | tf_op jit(solution)/shard_map/psum | solution.py:160
  298.5 3.8 fusion.44
  302.3 1.2 copy-done.18
  303.5 5.6 %fusion.2 = bf16[1,2048,448]{1,2,0:T(8,128)(2,1)} fusion(bf16[1024,448]{0,1:T(8,128)(2,1)S(1)} %copy-done.18, bf16[1024,2048]{1,0:T(8,128)(2,1)} %bitcast.127), kind=kOutput, calls=%fused_computation.15 | convolution fusion | flops 1879965696 | bytes 6946816 | tf_op jit(solution)/shard_map/rd,rf->df/dot_general | solution.py:52
  309.1 3.4 fusion
  312.5 4.0 all-gather.10.cloned.1.call-done
  316.5 2.0 fusion.43
  318.8 0.1 slice.248
  318.9 0.1 slice.252
  320.8 0.2 slice.243
  321.3 0.1 rev.8
  321.6 0.1 rev.9
  321.8 27.2 %all-gather = f32[8,1,512]{2,1,0:T(1,128)S(1)} all-gather(f32[1,1,512]{2,1,0:T(1,128)S(1)} %get-tuple-element.113), channel_id=1, replica_groups=mesh['sp'=8,'tp'=4] {'sp'}, dimensions={0}, use_global_device_ids=true | all-gather | bytes 18432 | tf_op jit(solution)/shard_map/all_gather | solution.py:13
  349.0 26.6 %all-gather.1 = f32[8,1,512]{2,1,0:T(1,128)S(1)} all-gather(f32[1,1,512]{2,1,0:T(1,128)S(1)} %get-tuple-element.112), channel_id=1, replica_groups=mesh['sp'=8,'tp'=4] {'sp'}, dimensions={0}, use_global_device_ids=true | all-gather | bytes 18432 | tf_op jit(solution)/shard_map/all_gather | solution.py:13
  375.7 0.3 while.14
  376.0 0.5 fusion.34
  376.5 0.2 convolution_bitcast_fusion
  376.8 0.2 convolution_bitcast_fusion.1
  377.1 0.8 add_add_fusion
  377.9 30.1 %reduce-scatter.2.cloned.1.call-done = f32[256,512]{1,0:T(8,128)} async-done(((f32[2048,512]{1,0:T(8,128)}), f32[256,512]{1,0:T(8,128)}) %reduce-scatter.2.cloned.1.call-update) | async-done | bytes 524304 | tf_op jit(solution)/shard_map/reduce_scatter | solution.py:231
  (191 shorter events, 3.5 us)
Async XLA Ops:
  8.0 91.2 %copy-start = (bf16[1,2048,448]{1,2,0:T(8,128)(2,1)S(1)}, bf16[1,2048,448]{1,2,0:T(8,128)(2,1)}, u32[]{:S(2)}) copy-start(bf16[1,2048,448]{1,2,0:T(8,128)(2,1)} %param.22) | copy-start | bytes 5505028
  8.0 91.2 %all-gather.6.cloned.1.call-start = ((), (), s32[]{:S(2)}) async-start(), calls=%async_computation.4 | async-start | bytes 5242880 | tf_op jit(solution)/shard_map/all_gather | solution.py:141
  22.3 33.4 %copy-start.2 = (bf16[128,2048]{1,0:T(8,128)(2,1)S(1)}, bf16[128,2048]{1,0:T(8,128)(2,1)}, u32[]{:S(2)}) copy-start(bf16[128,2048]{1,0:T(8,128)(2,1)} %param.18) | copy-start | bytes 1572868
  55.6 77.2 %all-gather.8.cloned.1.call-start = ((), (), s32[]{:S(2)}) async-start(), calls=%async_computation.5 | async-start | bytes 5242880 | tf_op jit(solution)/shard_map/all_gather | solution.py:140
  58.1 3.8 copy-start.11
  99.2 5.7 %copy-start.12 = (bf16[8,128,2048]{2,1,0:T(8,128)(2,1)S(1)}, bf16[8,128,2048]{2,1,0:T(8,128)(2,1)}, u32[]{:S(2)}) copy-start(bf16[8,128,2048]{2,1,0:T(8,128)(2,1)} %all-gather.6.cloned.1.call-done) | copy-start | bytes 12582916
  99.2 5.7 %copy-start.14 = (bf16[1,2048,448]{1,2,0:T(8,128)(2,1)S(1)}, bf16[1,2048,448]{1,2,0:T(8,128)(2,1)}, u32[]{:S(2)}) copy-start(bf16[1,2048,448]{1,2,0:T(8,128)(2,1)} %param.23) | copy-start | bytes 5505028
  139.2 2.5 copy-start.16
  139.2 2.5 copy-start.17
  139.2 2.5 copy-start.15
  146.2 99.2 %all-to-all-start.2 = ((bf16[8,128,2048]{2,1,0:T(8,128)(2,1)}), bf16[8,128,2048]{2,1,0:T(8,128)(2,1)}, u32[]{:S(2)}, u32[]{:S(2)}) async-start(bf16[8,128,2048]{2,1,0:T(8,128)(2,1)} %bitcast.105), calls=%async_computation.2 | async-start | bytes 8388608 | tf_op jit(solution)/shard_map/all_to_all | solution.py:152
  151.7 146.8 %all-reduce.32.cloned.1.call-start = ((), (), s32[]{:S(2)}) async-start(), calls=%async_computation.6 | async-start | bytes 1048576 | tf_op jit(solution)/shard_map/psum | solution.py:160
  261.7 5.9 %copy-start.6 = (bf16[2,256,256]{2,1,0:T(8,128)(2,1)S(1)}, bf16[2,256,256]{2,1,0:T(8,128)(2,1)}, u32[]{:S(2)}) copy-start(bf16[2,256,256]{2,1,0:T(8,128)(2,1)} %param.30) | copy-start | bytes 786436
  261.7 6.0 %copy-start.7 = (bf16[128,512]{1,0:T(8,128)(2,1)S(1)}, bf16[128,512]{1,0:T(8,128)(2,1)}, u32[]{:S(2)}) copy-start(bf16[128,512]{1,0:T(8,128)(2,1)} %param.26) | copy-start | bytes 393220
  266.8 1.4 copy-start.9
  266.8 1.4 copy-start.10
  266.8 49.7 %all-gather.10.cloned.1.call-start = ((), (), s32[]{:S(2)}) async-start(), calls=%async_computation.8 | async-start | bytes 2359296 | tf_op jit(solution)/shard_map/all_gather | solution.py:166
  267.4 140.6 %reduce-scatter.2.cloned.1.call-start = ((), (), s32[]{:S(2)}) async-start(), calls=%async_computation.7 | async-start | bytes 4718592 | tf_op jit(solution)/shard_map/reduce_scatter | solution.py:231
  267.7 1.0 copy-start.5
  269.5 29.0 %copy-start.4 = (bf16[128,512]{1,0:T(8,128)(2,1)S(1)}, bf16[128,512]{1,0:T(8,128)(2,1)}, u32[]{:S(2)}) copy-start(bf16[128,512]{1,0:T(8,128)(2,1)} %param.27) | copy-start | bytes 393220
  302.3 1.2 copy-start.18
  303.5 5.6 %copy-start.13 = (bf16[8,128,2048]{2,1,0:T(8,128)(2,1)S(1)}, bf16[8,128,2048]{2,1,0:T(8,128)(2,1)}, u32[]{:S(2)}) copy-start(bf16[8,128,2048]{2,1,0:T(8,128)(2,1)} %all-gather.8.cloned.1.call-done) | copy-start | bytes 12582916
  303.5 5.6 %copy-start.19 = (f32[1024,448]{0,1:T(8,128)S(1)}, f32[1024,448]{0,1:T(8,128)}, u32[]{:S(2)}) copy-start(f32[1024,448]{0,1:T(8,128)} %fusion.5) | copy-start | bytes 5505028
  303.5 5.6 %copy-start.20 = (f32[1024,448]{0,1:T(8,128)S(1)}, f32[1024,448]{0,1:T(8,128)}, u32[]{:S(2)}) copy-start(f32[1024,448]{0,1:T(8,128)} %fusion.8) | copy-start | bytes 5505028
  309.1 7.4 %copy-start.3 = (bf16[128,2048]{1,0:T(8,128)(2,1)S(1)}, bf16[128,2048]{1,0:T(8,128)(2,1)}, u32[]{:S(2)}) copy-start(bf16[128,2048]{1,0:T(8,128)(2,1)} %all-reduce.32.cloned.1.call-done) | copy-start | bytes 1572868
  321.3 54.7 %copy-start.8 = (bf16[128,512]{1,0:T(8,128)(2,1)S(1)}, bf16[128,512]{1,0:T(8,128)(2,1)}, u32[]{:S(2)}) copy-start(bf16[128,512]{1,0:T(8,128)(2,1)} %param.26) | copy-start | bytes 393220
  376.5 31.4 %copy-start.1 = (bf16[1,2048,448]{1,2,0:T(8,128)(2,1)S(1)}, bf16[1,2048,448]{1,2,0:T(8,128)(2,1)}, u32[]{:S(2)}) copy-start(bf16[1,2048,448]{1,2,0:T(8,128)(2,1)} %param.22) | copy-start | bytes 5505028
Sparse Core Ops, SparseCore 0:
  55.7 33.4 all-gather.5
  99.3 33.4 all-gather.7
  266.9 31.5 all-reduce.31
Sparse Core Ops, SparseCore 1:
  269.4 47.0 all-gather.9
  320.6 87.3 reduce-scatter.1
where the time goes:
time: 423 us; the launch traced here: 415 us
  waiting for transfers between devices  176 us (42%)
  blocking collectives  117 us (28%)
  matrix products  44.1 us (10%)
  local copies, waits for them, and re-layouts  37.3 us (9%)
  other arithmetic  18.9 us (4%)
  between operations  16.7 us (4%)
  starting transfers between devices  6.18 us (1%)
    all_to_all x1, waiting for transfers between devices, local(): lax.all_to_all(token_part.astype(jnp.bfloat16).reshape(sp_count, capacity...  93.4 us
    all_gather x2, blocking collectives, prefix(): gathered = jax.tree.map(lambda a: lax.all_gather(a, axis), part)  53.9 us
    all_to_all x1, blocking collectives, local(): lax.all_to_all(send_rows.reshape(sp_count, capacity, share), 'sp', split_...  33.3 us
    reduce_scatter x1, waiting for transfers between devices, local(): lax.psum_scatter(jnp.einsum('tr,tc->rc', columns, memory_hidden_values, p...  30.1 us
    all_to_all x1, blocking collectives, local(): lax.all_to_all(send_grad.reshape(sp_count, capacity, share), 'sp', split_...  29.4 us
    all_gather x1, waiting for transfers between devices, local(): lax.all_gather(got_grad, 'tp', axis=2, tiled=True)  24.5 us
    psum x1, waiting for transfers between devices, local(): moe_grad = lax.psum(own_sum.astype(jnp.bfloat16), 'tp').astype(jnp.float32)  23.1 us
  transfers between devices with their start and end apart: 6, of which 5 were waited for; matrix products, arithmetic and copies ran while one was open for 12% of the time, Pallas kernels for 0%

commit v1 on v0

--- a/solution.py
+++ b/solution.py
@@ -1,6 +1,10 @@
+import functools
+
 import jax
 import jax.numpy as jnp
 from jax import lax
+from jax.experimental import pallas as pl
+from jax.experimental.pallas import tpu as pltpu
 from jax.sharding import PartitionSpec as P
 
 SLICES = 2
@@ -71,6 +75,208 @@
     for target in targets:
         buffer = buffer.at[target].set(values)
     return buffer
+
+
+MESH_ID = pl.DeviceIdType.MESH
+
+
+def greet(peers):
+    barrier = pltpu.get_barrier_semaphore()
+    for peer in peers:
+        pl.semaphore_signal(barrier, inc=1, device_id=peer, device_id_type=MESH_ID)
+    pl.semaphore_wait(barrier, len(peers))
+
+
+def remote(src, dst, send, recv, peer):
+    return pltpu.make_async_remote_copy(
+        src_ref=src, dst_ref=dst, send_sem=send, recv_sem=recv, device_id=peer, device_id_type=MESH_ID
+    )
+
+
+def places(sp_count):
+    me = lax.axis_index("sp")
+    tp = lax.axis_index("tp")
+    side, core = tp // 2, tp % 2
+    peers = [(lax.rem(me + k, sp_count), tp) for k in range(sp_count)]
+    sources = [lax.rem(me + sp_count - k, sp_count) for k in range(sp_count)]
+    sibling = (me, side * 2 + (1 - core))
+    across = (me, (1 - side) * 2 + core)
+    return me, side, core, peers, sources, sibling, across
+
+
+def gather_kernel(sp_count, x_ref, g_ref, info_ref, r_ref, h_ref, xo, go, io, ro, ho,
+                  ds, dr, ys, yr, ss, sr, s2, r2, local_sem):
+    me, side, core, peers, sources, sibling, across = places(sp_count)
+    rows, feats = x_ref.shape
+    half = feats // 2
+    passed = 3 * half // 8
+    direct = half - passed
+    first = pl.multiple_of(core * half + side * passed, 128)
+    onward = pl.multiple_of(core * half + side * direct, 128)
+    back = pl.multiple_of(core * half + (1 - side) * direct, 128)
+
+    def at(ref, who, col, width):
+        return ref.at[pl.ds(pl.multiple_of(who * rows, rows), rows), pl.ds(col, width)]
+
+    def block(ref, who, size):
+        return ref.at[pl.ds(pl.multiple_of(who * size, size), size), :]
+
+    greet(peers[1:] + [sibling, across])
+    pairs = ((x_ref, xo), (g_ref, go))
+    small = ((info_ref, io), (r_ref, ro), (h_ref, ho))
+    waits = []
+    copies = {}
+    for a, (src, dst) in enumerate(pairs):
+        for k in range(1, sp_count):
+            cp = remote(src.at[:, pl.ds(first, direct)], at(dst, me, first, direct), ds.at[a, k], dr.at[a, k], peers[k])
+            cp.start()
+            copies[a, k] = cp
+    for b, (src, dst) in enumerate(small):
+        for k in range(1, sp_count):
+            cp = remote(src, block(dst, me, src.shape[0]), s2.at[b, k], r2.at[b, k], peers[k])
+            cp.start()
+            waits.append(cp)
+    locals_ = []
+    for n, (src, dst) in enumerate(pairs + small):
+        cp = pltpu.make_async_copy(src, block(dst, me, src.shape[0]), local_sem.at[n])
+        cp.start()
+        locals_.append(cp)
+    for a, (src, dst) in enumerate(pairs):
+        for k in range(1, sp_count):
+            who = sources[k]
+            copies[a, k].wait_recv()
+            cp = remote(at(dst, who, onward, passed), at(dst, who, onward, passed), ys.at[a, k], yr.at[a, k], across)
+            cp.start()
+            copies[a, k, 1] = cp
+            cp = remote(at(dst, who, first, direct), at(dst, who, first, direct), ss.at[a, k, 0], sr.at[a, k, 0], sibling)
+            cp.start()
+            waits.append(cp)
+    for a, (src, dst) in enumerate(pairs):
+        for k in range(1, sp_count):
+            who = sources[k]
+            copies[a, k, 1].wait_recv()
+            cp = remote(at(dst, who, back, passed), at(dst, who, back, passed), ss.at[a, k, 1], sr.at[a, k, 1], sibling)
+            cp.start()
+            waits.append(cp)
+    for a in range(2):
+        for k in range(1, sp_count):
+            copies[a, k].wait_send()
+            copies[a, k, 1].wait_send()
+    for cp in waits + locals_:
+        cp.wait()
+
+
+def gather_all(sp_count, x, g, info, r, h):
+    dma = pltpu.SemaphoreType.DMA
+    outs = [jax.ShapeDtypeStruct((a.shape[0] * sp_count, a.shape[1]), a.dtype) for a in (x, g, info, r, h)]
+    return pl.pallas_call(
+        functools.partial(gather_kernel, sp_count),
+        out_shape=outs,
+        in_specs=[pl.BlockSpec(memory_space=pltpu.VMEM)] * 5,
+        out_specs=[pl.BlockSpec(memory_space=pl.ANY)] * 5,
+        scratch_shapes=[dma((2, sp_count))] * 4 + [dma((2, sp_count, 2))] * 2 + [dma((3, sp_count))] * 2 + [dma((5,))],
+        compiler_params=pltpu.CompilerParams(collective_id=0, has_side_effects=True),
+    )(x, g, info, r, h)
+
+
+def return_kernel(sp_count, p_ref, g_ref, mixed, cols_out, sib, out, got, ybuf, yown,
+                  a_s, a_r, b_s, b_r, c_s, c_r, d_s, d_r, local_sem):
+    me, side, core, peers, sources, sibling, across = places(sp_count)
+    rows, feats = g_ref.shape
+    half = feats // 2
+    mine = pl.multiple_of(core * half, half)
+    theirs = pl.multiple_of((1 - core) * half, half)
+    greet(peers[1:] + [sibling, across])
+    order = list(range(1, sp_count)) + [0]
+    first = {}
+    for k in order:
+        at = pl.ds(pl.multiple_of(peers[k][0] * rows, rows), rows)
+        first[k] = remote(p_ref.at[at, pl.ds(theirs, half)], sib.at[k], a_s.at[k], a_r.at[k], sibling)
+        first[k].start()
+    second = {}
+    for k in order:
+        at = pl.ds(pl.multiple_of(peers[k][0] * rows, rows), rows)
+        first[k].wait_recv()
+        total = p_ref[at, pl.ds(mine, half)].astype(jnp.float32) + sib[k].astype(jnp.float32)
+        out[k] = total.astype(jnp.bfloat16)
+        if k:
+            second[k] = remote(out.at[k], got.at[k], b_s.at[k], b_r.at[k], peers[k])
+            second[k].start()
+    total = out[0].astype(jnp.float32)
+    for k in range(1, sp_count):
+        second[k].wait_recv()
+        total = total + got[k].astype(jnp.float32)
+    yown[...] = total.astype(jnp.bfloat16)
+    cross = remote(yown, ybuf, c_s.at[0], c_r.at[0], across)
+    cross.start()
+    cross.wait()
+    part = pl.ds(mine, half)
+    total = yown[...].astype(jnp.float32) + ybuf[...].astype(jnp.float32)
+    mixed[:, part] = (g_ref[:, part].astype(jnp.float32) + total).astype(jnp.bfloat16)
+    share = remote(mixed.at[:, part], mixed.at[:, part], c_s.at[1], c_r.at[1], sibling)
+    share.start()
+    share.wait()
+    width = feats // sp_count
+    own = pl.ds(pl.multiple_of(me * rows, rows), rows)
+    last = []
+    for k in range(1, sp_count):
+        cols = pl.ds(pl.multiple_of(peers[k][0] * width, width), width)
+        cp = remote(mixed.at[:, cols], cols_out.at[own, :], d_s.at[k], d_r.at[k], peers[k])
+        cp.start()
+        last.append(cp)
+    here = pltpu.make_async_copy(mixed.at[:, pl.ds(pl.multiple_of(me * width, width), width)], cols_out.at[own, :], local_sem)
+    here.start()
+    here.wait()
+    for cp in last:
+        cp.wait()
+    for k in order:
+        first[k].wait_send()
+    for k in range(1, sp_count):
+        second[k].wait_send()
+
+
+def return_all(sp_count, partial, g):
+    dma = pltpu.SemaphoreType.DMA
+    rows, feats = g.shape
+    half = feats // 2
+    big = pltpu.VMEM((sp_count, rows, half), jnp.bfloat16)
+    one = pltpu.VMEM((rows, half), jnp.bfloat16)
+    return pl.pallas_call(
+        functools.partial(return_kernel, sp_count),
+        out_shape=[
+            jax.ShapeDtypeStruct((rows, feats), jnp.bfloat16),
+            jax.ShapeDtypeStruct((rows * sp_count, feats // sp_count), jnp.bfloat16),
+        ],
+        in_specs=[pl.BlockSpec(memory_space=pltpu.VMEM)] * 2,
+        out_specs=[pl.BlockSpec(memory_space=pltpu.VMEM)] * 2,
+        scratch_shapes=[big, big, big, one, one] + [dma((sp_count,))] * 4 + [dma((2,))] * 2 + [dma((sp_count,))] * 2 + [dma],
+        compiler_params=pltpu.CompilerParams(collective_id=1, has_side_effects=True),
+    )(partial, g)
+
+
+def carry_kernel(sp_count, c_ref, got, s, r):
+    me, side, core, peers, sources, sibling, across = places(sp_count)
+    greet(peers[1:])
+    copies = []
+    for k in range(1, sp_count):
+        cp = remote(c_ref, got.at[me], s.at[k], r.at[k], peers[k])
+        cp.start()
+        copies.append(cp)
+    got[me] = c_ref[...]
+    for cp in copies:
+        cp.wait()
+
+
+def carry_all(sp_count, block):
+    dma = pltpu.SemaphoreType.DMA
+    return pl.pallas_call(
+        functools.partial(carry_kernel, sp_count),
+        out_shape=jax.ShapeDtypeStruct((sp_count,) + block.shape, block.dtype),
+        in_specs=[pl.BlockSpec(memory_space=pltpu.VMEM)],
+        out_specs=pl.BlockSpec(memory_space=pltpu.VMEM),
+        scratch_shapes=[dma((sp_count,))] * 2,
+        compiler_params=pltpu.CompilerParams(collective_id=2, has_side_effects=True),
+    )(block)
 
 
 def local(
@@ -243,9 +449,141 @@
     )
 
 
+def direct(
+    result_cotangent_values,
+    specialist_entry_vectors,
+    chosen_specialists,
+    specialist_mixing_shares,
+    specialist_switch_maps,
+    specialist_widen_maps,
+    specialist_shrink_maps,
+    memory_readout_map,
+    memory_source_vectors,
+    memory_hidden_values,
+    feature_fading_speed,
+    extra_log_fading,
+    memory_switch_tiles,
+    entry_switch_tiles,
+):
+    tok_rows, feature_count = result_cotangent_values.shape
+    sp_count = lax.axis_size("sp")
+    info = jnp.concatenate(
+        [
+            chosen_specialists.astype(jnp.float32).T,
+            specialist_mixing_shares.T,
+            jnp.zeros((4, tok_rows), jnp.float32),
+        ],
+        axis=0,
+    )
+    inputs, all_grad, info, readout, hidden_all = gather_all(
+        sp_count,
+        specialist_entry_vectors,
+        result_cotangent_values,
+        info,
+        memory_readout_map,
+        memory_hidden_values,
+    )
+    expert = (lax.axis_index("sp") // SLICES).astype(jnp.float32)
+    info = info.reshape(sp_count, 8, tok_rows)
+    share = jnp.where(info[:, 0] == expert, info[:, 2], 0.0) + jnp.where(
+        info[:, 1] == expert, info[:, 3], 0.0
+    )
+    grads_in = (share.reshape(-1, 1) * all_grad.astype(jnp.float32)).astype(jnp.bfloat16)
+    gate_weight_grad, up_weight_grad, down_grad, token_part = expert_backward(
+        inputs,
+        grads_in,
+        specialist_switch_maps[0],
+        specialist_widen_maps[0],
+        specialist_shrink_maps[0],
+    )
+    mixed_grad, mixed_cols = return_all(
+        sp_count, token_part.astype(jnp.bfloat16), result_cotangent_values
+    )
+    col_count = memory_readout_map.shape[1]
+    upstream = jnp.dot(mixed_grad, readout, preferred_element_type=jnp.float32)
+    blocks_here = memory_switch_tiles.shape[0]
+    block_width = memory_switch_tiles.shape[1]
+    blocks_in = memory_source_vectors.reshape(tok_rows, blocks_here, block_width)
+    memory_switch_fraction = jax.nn.sigmoid(
+        jnp.einsum(
+            "tnc,ncd->tnd", blocks_in, memory_switch_tiles, preferred_element_type=jnp.float32
+        ).reshape(tok_rows, col_count)
+    )
+    inp_open = jax.nn.sigmoid(
+        jnp.einsum(
+            "tnc,ncd->tnd", blocks_in, entry_switch_tiles, preferred_element_type=jnp.float32
+        ).reshape(tok_rows, col_count)
+    )
+    xin = memory_source_vectors.astype(jnp.float32)
+    log_fading_factor = (
+        -8.0 * memory_switch_fraction * feature_fading_speed[None, :] + extra_log_fading[:, None]
+    )
+    decay_mult = jnp.exp(log_fading_factor)
+    spare_room = -jnp.expm1(2.0 * log_fading_factor)
+    in_scale = jnp.sqrt(jnp.maximum(spare_room, 0.01))
+    drive = in_scale * inp_open * xin
+    coeff = jnp.concatenate([decay_mult[1:], jnp.ones((1, col_count), jnp.float32)], axis=0)
+    prod_after, local_part = lax.associative_scan(compose, (coeff, upstream), reverse=True, axis=0)
+    alpha_part = decay_mult[0] * local_part[0]
+    beta_part = decay_mult[0] * prod_after[0]
+    gathered = carry_all(
+        sp_count,
+        jnp.concatenate(
+            [beta_part[None], alpha_part[None], jnp.zeros((6, col_count), jnp.float32)], axis=0
+        ),
+    )
+    place = lax.axis_index("sp")
+    incoming = jnp.zeros((col_count,), jnp.float32)
+    for source in range(sp_count - 1, 0, -1):
+        incoming = jnp.where(
+            source > place, gathered[source, 1] + gathered[source, 0] * incoming, incoming
+        )
+    dstate = local_part + prod_after * incoming[None, :]
+    scale_slope = jnp.where(spare_room > 0.01, -decay_mult * decay_mult / in_scale, 0.0)
+    log_grad = dstate * (
+        memory_hidden_values.astype(jnp.float32) - drive + scale_slope * inp_open * xin
+    )
+    grad_rec = (
+        log_grad
+        * (-8.0 * feature_fading_speed[None, :])
+        * memory_switch_fraction
+        * (1.0 - memory_switch_fraction)
+    ).astype(jnp.bfloat16)
+    grad_in = (dstate * in_scale * xin * inp_open * (1.0 - inp_open)).astype(jnp.bfloat16)
+    back_rec = jnp.einsum(
+        "tnd,ncd->tnc",
+        grad_rec.reshape(tok_rows, blocks_here, block_width),
+        memory_switch_tiles,
+        preferred_element_type=jnp.float32,
+    )
+    back_in = jnp.einsum(
+        "tnd,ncd->tnc",
+        grad_in.reshape(tok_rows, blocks_here, block_width),
+        entry_switch_tiles,
+        preferred_element_type=jnp.float32,
+    )
+    lru_input_grad = (
+        dstate * in_scale * inp_open
+        + back_rec.reshape(tok_rows, col_count)
+        + back_in.reshape(tok_rows, col_count)
+    )
+    out_proj_grad = jnp.einsum(
+        "tr,tc->rc", mixed_cols, hidden_all, preferred_element_type=jnp.float32
+    )
+    return (
+        gate_weight_grad[None],
+        up_weight_grad[None],
+        down_grad[None],
+        out_proj_grad,
+        lru_input_grad,
+    )
+
+
 def solution(mesh):
+    sp_count, tp_count = mesh.shape["sp"], mesh.shape["tp"]
+    whole_blocks = 4 * SLICES == sp_count and tp_count == 4
     return jax.shard_map(
-        local,
+        direct if whole_blocks else local,
         mesh=mesh,
         in_specs=(
             P("sp", None),

time: 423 us -> 288 us (0.68); the launches traced: 415 us -> 287 us
  Pallas kernels: 0 us -> 221 us
  waiting for transfers between devices: 176 us -> 0 us
  blocking collectives: 117 us -> 0 us
  local copies, waits for them, and re-layouts: 37.3 us -> 12.4 us
  between operations: 16.7 us -> 1.47 us
  starting transfers between devices: 6.18 us -> 0 us
  matrix products: 44.1 us -> 38.6 us
  other arithmetic: 18.9 us -> 13.6 us
    pallas_call x0 -> x3, Pallas kernels: none -> 221 us  [the longest x1 127 us: gather_all(): pl.pallas_call(functools.partial(gather_kernel, sp_count), out_shape=outs...]
    all_to_all x1 -> x0, waiting for transfers between devices: 93.4 us -> none  [local(): lax.all_to_all(token_part.astype(jnp.bfloat16).reshape(sp_count, capacity...]
    all_to_all x2 -> x0, blocking collectives: 62.7 us -> none  [the longest x1 33.3 us: local(): lax.all_to_all(send_rows.reshape(sp_count, capacity, share), 'sp', split_...]
    all_gather x2 -> x0, blocking collectives: 53.9 us -> none  [prefix(): gathered = jax.tree.map(lambda a: lax.all_gather(a, axis), part)]
    reduce_scatter x1 -> x0, waiting for transfers between devices: 30.1 us -> none  [local(): lax.psum_scatter(jnp.einsum('tr,tc->rc', columns, memory_hidden_values, p...]
    all_gather x3 -> x0, waiting for transfers between devices: 28.5 us -> none  [the longest x1 24.5 us: local(): lax.all_gather(got_grad, 'tp', axis=2, tiled=True)]
    psum x1 -> x0, waiting for transfers between devices: 23.1 us -> none  [local(): moe_grad = lax.psum(own_sum.astype(jnp.bfloat16), 'tp').astype(jnp.float32)]
    gather x2 -> x0, local copies, waits for them, and re-layouts: 12.1 us -> none  [the longest x1 6.06 us: collect(): gathered = gathered + jnp.take(returned, target, axis=0).astype(jnp.float32)]
  transfers between devices with their start and end apart: 6 -> 0, of which waited for: 5 -> 0; matrix products, arithmetic and copies ran while one was open for 12% -> 0% of each run, Pallas kernels for 0% -> 0%
where the time goes in v1:
time: 288 us; the launch traced here: 287 us
  Pallas kernels  221 us (77%)
  matrix products  38.6 us (13%)
  other arithmetic  13.6 us (5%)
  local copies, waits for them, and re-layouts  12.4 us (4%)
    pallas_call x1, Pallas kernels, gather_all(): pl.pallas_call(functools.partial(gather_kernel, sp_count), out_shape=outs...  127 us
    pallas_call x1, Pallas kernels, return_all(): pl.pallas_call(functools.partial(return_kernel, sp_count), out_shape=[jax...  82.3 us
    pallas_call x1, Pallas kernels, carry_all(): pl.pallas_call(functools.partial(carry_kernel, sp_count), out_shape=jax.S...  11.9 us
    dot_general x1, matrix products, expert_backward(): jnp.einsum('rd,fd->rf', grads_in, down_weight, preferred_element_type=jnp...  6.64 us

profile of v1, /device:TPU:0, one launch (start us, length us, event | category | flops | bytes accessed | tf_op | source)
XLA Modules:
  0.0 287.5 jit_solution(18362249565073499458)
XLA Ops:
  0.6 0.0 copy-start
  0.6 0.8 convert_bitcast_fusion
  1.5 0.1 pad.145.clone
  1.5 1.3 maximum_maximum_fusion.1.info_ref
  2.9 127.2 %shard_map.173 = (bf16[1024,2048]{1,0:T(8,128)(2,1)}, bf16[1024,2048]{1,0:T(8,128)(2,1)}, f32[64,128]{1,0:T(8,128)}, bf16[2048,512]{1,0:T(8,128)(2,1)}, bf16[1024,512]{1,0:T(8,128)(2,1)}) custom-call(bf16[128,2048]{1,0:T(8,128)(2,1)} %x_ref.1, bf16[128,2048]{1,0:T(8,128)(2,1)} %g_ref.3, f32[8,128]{1,0:T(8,128)} %maximum_maximum_fusion.1.info_ref, ...), custom_call_target="tpu_custom_call" | custom-call | tf_op jit(solution)/shard_map/pallas_call | solution.py:172
  130.1 0.0 copy-done
  130.1 0.0 copy-start.13
  130.1 0.0 copy-start.15
  130.1 5.7 %fusion.5 = f32[1024,448]{0,1:T(8,128)} fusion(bf16[1024,2048]{1,0:T(8,128)(2,1)} %get-tuple-element.12, bf16[1,2048,448]{1,2,0:T(8,128)(2,1)S(1)} %copy-done), kind=kOutput, calls=%fused_computation.10 | convolution fusion | flops 1879048192 | bytes 7864320 | tf_op jit(solution)/shard_map/dot_general | solution.py:43
  135.8 0.0 copy-done.13
  135.8 3.4 %fusion.8 = f32[1024,448]{0,1:T(8,128)} fusion(bf16[1024,2048]{1,0:T(8,128)(2,1)S(1)} %copy-done.13, bf16[1,2048,448]{1,2,0:T(8,128)(2,1)S(1)} %copy-done.15), kind=kOutput, calls=%fused_computation.13 | convolution fusion | flops 1879048192 | bytes 7864320 | tf_op jit(solution)/shard_map/dot_general | solution.py:44
  139.2 6.6 %multiply_convert_fusion.2 = (bf16[1024,448]{0,1:T(8,128)(2,1)S(1)}, bf16[1024,448]{0,1:T(8,128)(2,1)S(1)}) fusion(f32[1024,448]{0,1:T(8,128)} %fusion.5, f32[1024,448]{0,1:T(8,128)} %fusion.8, bf16[1,448,2048]{2,1,0:T(8,128)(2,1)} %param.20, bf16[1024,2048]{1,0:T(8,128)(2,1)} %get-tuple-element.14, f32[1024]{0:T(1024)S(1)} %bitcast.105), kind=kOutput, calls=%fused_computation.18 | convolution fusion | flops 1891303424 | bytes 11538432 | tf_op jit(solution)/shard_map/rd,fd->rf/dot_general | solution.py:50
  145.8 3.3 %fusion.1 = bf16[1,2048,448]{1,2,0:T(8,128)(2,1)} fusion(bf16[1024,448]{0,1:T(8,128)(2,1)S(1)} %get-tuple-element.22, bf16[1024,2048]{1,0:T(8,128)(2,1)S(1)} %copy-done.14), kind=kOutput, calls=%fused_computation.6 | convolution fusion | flops 1879965696 | bytes 6946816 | tf_op jit(solution)/shard_map/rd,rf->df/dot_general | solution.py:53
  149.1 3.3 %fusion.2 = bf16[1,2048,448]{1,2,0:T(8,128)(2,1)} fusion(bf16[1024,448]{0,1:T(8,128)(2,1)S(1)} %get-tuple-element.21, bf16[1024,2048]{1,0:T(8,128)(2,1)S(1)} %copy-done.14), kind=kOutput, calls=%fused_computation.7 | convolution fusion | flops 1879965696 | bytes 6946816 | tf_op jit(solution)/shard_map/rd,rf->df/dot_general | solution.py:56
  152.4 0.5 copy-done.18
  153.0 3.7 %fusion = bf16[1,448,2048]{2,1,0:T(8,128)(2,1)} fusion(bf16[1024,2048]{1,0:T(8,128)(2,1)S(1)} %copy-done.12, f32[1024]{0:T(1024)S(1)} %bitcast.106, f32[1024,448]{0,1:T(8,128)S(1)} %copy-done.18, f32[1024,448]{0,1:T(8,128)S(1)} %copy-done.17), kind=kOutput, calls=%fused_computation.5 | convolution fusion | flops 1889009664 | bytes 9703424 | tf_op jit(solution)/shard_map/rf,rd->fd/dot_general | solution.py:47
  156.7 2.4 fusion.3
  159.1 4.6 %add_convert_fusion.p_ref = bf16[1024,2048]{1,0:T(8,128)(2,1)} fusion(f32[1024,2048]{1,0:T(8,128)S(1)} %fusion.3, bf16[1024,448]{0,1:T(8,128)(2,1)S(1)} %get-tuple-element.21, bf16[1,2048,448]{1,2,0:T(8,128)(2,1)S(1)} %copy-done.16), kind=kOutput, calls=%fused_computation | convolution fusion | flops 1883242496 | bytes 15335424 | tf_op jit(solution)/shard_map/rf,df->rd/dot_general | solution.py:60
  163.7 82.3 %shard_map.174 = (bf16[128,2048]{1,0:T(8,128)(2,1)}, bf16[1024,256]{1,0:T(8,128)(2,1)}) custom-call(bf16[1024,2048]{1,0:T(8,128)(2,1)} %add_convert_fusion.p_ref, bf16[128,2048]{1,0:T(8,128)(2,1)} %g_ref.3), custom_call_target="tpu_custom_call" | custom-call | tf_op jit(solution)/shard_map/pallas_call | solution.py:244
  246.1 0.0 copy-start.4
  246.1 0.0 copy-start.8
  246.1 0.0 copy-start.6
  246.1 2.4 fusion.63
  248.5 0.3 fusion.15
  248.8 0.1 copy.32
  248.9 0.3 fusion.18
  249.2 0.1 copy.31
  249.4 0.1 fusion.33
  249.5 0.7 copy-done.1
  250.3 0.1 slice.295
  250.4 1.3 slice.296
  251.7 0.1 slice.299
  251.8 0.1 slice.300
  251.9 0.1 slice.305
  252.0 0.1 slice.306
  252.1 2.2 fusion.64
  254.4 0.1 slice.297
  254.5 0.1 slice.298
  254.6 0.1 slice.301
  254.7 0.1 slice.302
  256.0 0.0 copy-start.3
  256.0 0.6 add_multiply_fusion.4
  256.8 0.6 slice.304
  257.5 0.8 pad_maximum_fusion.3
  258.3 1.5 add_multiply_fusion.2
  259.8 0.1 slice.292
  259.9 1.3 slice.293
  261.3 0.9 pad_maximum_fusion.1
  262.2 1.6 add_multiply_fusion
  264.0 1.3 rev.8
  265.3 0.9 concatenate.58
  266.4 0.7 add.282
  267.1 3.0 %rev.9 = f32[128,512]{1,0:T(8,128)} reverse(f32[128,512]{1,0:T(8,128)} %add.282), dimensions={0} | reverse | bytes 524288 | tf_op jit(solution)/shard_map/rev | solution.py:526
  270.1 0.7 add_multiply_fusion.11
  270.8 0.0 copy-start.5
  270.8 0.0 copy-start.7
  270.8 0.1 pad.120.clone
  270.9 0.7 maximum_maximum_fusion.c_ref
  271.6 11.9 %shard_map.175 = f32[8,8,512]{2,1,0:T(8,128)} custom-call(f32[8,512]{1,0:T(8,128)} %maximum_maximum_fusion.c_ref), custom_call_target="tpu_custom_call" | custom-call | tf_op jit(solution)/shard_map/pallas_call | solution.py:272
  283.5 1.0 fusion.55
  284.5 1.6 fusion.29
  286.2 0.2 convolution_bitcast_fusion
  286.4 0.2 convolution_bitcast_fusion.1
  286.7 0.8 add_add_fusion
  (124 shorter events, 1.6 us)
Async XLA Ops:
  0.6 129.4 %copy-start = (bf16[1,2048,448]{1,2,0:T(8,128)(2,1)S(1)}, bf16[1,2048,448]{1,2,0:T(8,128)(2,1)}, u32[]{:S(2)}) copy-start(bf16[1,2048,448]{1,2,0:T(8,128)(2,1)} %param.18) | copy-start | bytes 5505028
  130.1 5.7 %copy-start.13 = (bf16[1024,2048]{1,0:T(8,128)(2,1)S(1)}, bf16[1024,2048]{1,0:T(8,128)(2,1)}, u32[]{:S(2)}) copy-start(bf16[1024,2048]{1,0:T(8,128)(2,1)} %get-tuple-element.12) | copy-start | bytes 12582916
  130.1 5.7 %copy-start.15 = (bf16[1,2048,448]{1,2,0:T(8,128)(2,1)S(1)}, bf16[1,2048,448]{1,2,0:T(8,128)(2,1)}, u32[]{:S(2)}) copy-start(bf16[1,2048,448]{1,2,0:T(8,128)(2,1)} %param.19) | copy-start | bytes 5505028
  135.8 3.4 %copy-start.9 = (f32[64,128]{1,0:T(8,128)S(1)}, f32[64,128]{1,0:T(8,128)}, u32[]{:S(2)}) copy-start(f32[64,128]{1,0:T(8,128)} %get-tuple-element.13) | copy-start | bytes 98308
  139.1 6.7 %copy-start.14 = (bf16[1024,2048]{1,0:T(8,128)(2,1)S(1)}, bf16[1024,2048]{1,0:T(8,128)(2,1)}, u32[]{:S(2)}) copy-start(bf16[1024,2048]{1,0:T(8,128)(2,1)} %get-tuple-element.12) | copy-start | bytes 12582916
  149.1 3.3 %copy-start.12 = (bf16[1024,2048]{1,0:T(8,128)(2,1)S(1)}, bf16[1024,2048]{1,0:T(8,128)(2,1)}, u32[]{:S(2)}) copy-start(bf16[1024,2048]{1,0:T(8,128)(2,1)} %get-tuple-element.14) | copy-start | bytes 12582916
  149.1 3.3 %copy-start.17 = (f32[1024,448]{0,1:T(8,128)S(1)}, f32[1024,448]{0,1:T(8,128)}, u32[]{:S(2)}) copy-start(f32[1024,448]{0,1:T(8,128)} %fusion.5) | copy-start | bytes 5505028
  149.1 3.8 %copy-start.18 = (f32[1024,448]{0,1:T(8,128)S(1)}, f32[1024,448]{0,1:T(8,128)}, u32[]{:S(2)}) copy-start(f32[1024,448]{0,1:T(8,128)} %fusion.8) | copy-start | bytes 5505028
  156.7 2.4 copy-start.16
  163.7 82.4 %copy-start.2 = (bf16[1024,512]{1,0:T(8,128)(2,1)S(1)}, bf16[1024,512]{1,0:T(8,128)(2,1)}, u32[]{:S(2)}) copy-start(bf16[1024,512]{1,0:T(8,128)(2,1)} %get-tuple-element.16) | copy-start | bytes 3145732
  246.1 2.4 copy-start.4
  246.1 2.4 copy-start.8
  246.1 2.8 copy-start.6
  248.5 0.9 copy-start.10
  248.5 0.9 copy-start.11
  249.5 0.7 copy-start.1
  256.0 6.1 %copy-start.3 = (f32[63,512]{1,0:T(8,128)S(1)}, f32[63,512]{1,0:T(8,128)}, u32[]{:S(2)}) copy-start(f32[63,512]{1,0:T(8,128)} %slice.296) | copy-start | bytes 387076
  270.8 15.4 %copy-start.5 = (bf16[2,256,256]{2,1,0:T(8,128)(2,1)S(1)}, bf16[2,256,256]{2,1,0:T(8,128)(2,1)}, u32[]{:S(2)}) copy-start(bf16[2,256,256]{2,1,0:T(8,128)(2,1)} %param.27) | copy-start | bytes 786436
  270.8 15.6 %copy-start.7 = (bf16[2,256,256]{2,1,0:T(8,128)(2,1)S(1)}, bf16[2,256,256]{2,1,0:T(8,128)(2,1)}, u32[]{:S(2)}) copy-start(bf16[2,256,256]{2,1,0:T(8,128)(2,1)} %param.26) | copy-start | bytes 786436

commit v2 on v1

--- a/solution.py
+++ b/solution.py
@@ -105,8 +105,9 @@
 
 
 def gather_kernel(sp_count, x_ref, g_ref, info_ref, r_ref, h_ref, xo, go, io, ro, ho,
-                  ds, dr, ys, yr, ss, sr, s2, r2, local_sem):
+                  zs, zr, xs, xr, ys, yr, ss, sr, ts, tr, local_sem):
     me, side, core, peers, sources, sibling, across = places(sp_count)
+    tp = lax.axis_index("tp")
     rows, feats = x_ref.shape
     half = feats // 2
     passed = 3 * half // 8
@@ -114,6 +115,11 @@
     first = pl.multiple_of(core * half + side * passed, 128)
     onward = pl.multiple_of(core * half + side * direct, 128)
     back = pl.multiple_of(core * half + (1 - side) * direct, 128)
+    depth = sp_count // 2
+    z, x = me // 2, me % 2
+    partner = (z * 2 + 1 - x, tp)
+    along = [(lax.rem(z + k, depth) * 2 + x, tp) for k in range(depth)]
+    line = [lax.rem(z + depth - k, depth) * 2 for k in range(depth)]
 
     def at(ref, who, col, width):
         return ref.at[pl.ds(pl.multiple_of(who * rows, rows), rows), pl.ds(col, width)]
@@ -121,48 +127,79 @@
     def block(ref, who, size):
         return ref.at[pl.ds(pl.multiple_of(who * size, size), size), :]
 
-    greet(peers[1:] + [sibling, across])
+    greet(along[1:] + [partner, sibling, across])
     pairs = ((x_ref, xo), (g_ref, go))
     small = ((info_ref, io), (r_ref, ro), (h_ref, ho))
     waits = []
-    copies = {}
-    for a, (src, dst) in enumerate(pairs):
-        for k in range(1, sp_count):
-            cp = remote(src.at[:, pl.ds(first, direct)], at(dst, me, first, direct), ds.at[a, k], dr.at[a, k], peers[k])
-            cp.start()
-            copies[a, k] = cp
-    for b, (src, dst) in enumerate(small):
-        for k in range(1, sp_count):
-            cp = remote(src, block(dst, me, src.shape[0]), s2.at[b, k], r2.at[b, k], peers[k])
-            cp.start()
-            waits.append(cp)
-    locals_ = []
+    recv = {}
+
+    def send(key, src, dst, sems, index, peer):
+        cp = remote(src, dst, sems[0].at[index], sems[1].at[index], peer)
+        cp.start()
+        recv[key] = cp
+
     for n, (src, dst) in enumerate(pairs + small):
         cp = pltpu.make_async_copy(src, block(dst, me, src.shape[0]), local_sem.at[n])
         cp.start()
-        locals_.append(cp)
-    for a, (src, dst) in enumerate(pairs):
-        for k in range(1, sp_count):
-            who = sources[k]
-            copies[a, k].wait_recv()
-            cp = remote(at(dst, who, onward, passed), at(dst, who, onward, passed), ys.at[a, k], yr.at[a, k], across)
-            cp.start()
-            copies[a, k, 1] = cp
-            cp = remote(at(dst, who, first, direct), at(dst, who, first, direct), ss.at[a, k, 0], sr.at[a, k, 0], sibling)
-            cp.start()
-            waits.append(cp)
-    for a, (src, dst) in enumerate(pairs):
-        for k in range(1, sp_count):
-            who = sources[k]
-            copies[a, k, 1].wait_recv()
-            cp = remote(at(dst, who, back, passed), at(dst, who, back, passed), ss.at[a, k, 1], sr.at[a, k, 1], sibling)
-            cp.start()
-            waits.append(cp)
+        waits.append(cp)
+
+    def open_pair(a):
+        src, dst = pairs[a]
+        for k in range(depth - 1, 0, -1):
+            send(("z", a, k), src.at[:, pl.ds(first, direct)], at(dst, me, first, direct), (zs, zr), (a, k), along[k])
+        send(("x", a, 0), src.at[:, pl.ds(first, direct)], at(dst, me, first, direct), (xs, xr), (a, 0), partner)
+
+    def spread(a, who, n):
+        dst = pairs[a][1]
+        send(("y", a, n), at(dst, who, onward, passed), at(dst, who, onward, passed), (ys, yr), (a, n), across)
+        send(("s", a, n), at(dst, who, first, direct), at(dst, who, first, direct), (ss, sr), (a, n), sibling)
+
+    def open_small(b):
+        src, dst = small[b]
+        size = src.shape[0]
+        for k in range(depth - 1, 0, -1):
+            send(("z", 2 + b, k), src, block(dst, me, size), (zs, zr), (2 + b, k), along[k])
+        send(("x", 2 + b, 0), src, block(dst, me, size), (xs, xr), (2 + b, 0), partner)
+
+    open_pair(0)
+    open_small(0)
+    open_pair(1)
     for a in range(2):
-        for k in range(1, sp_count):
-            copies[a, k].wait_send()
-            copies[a, k, 1].wait_send()
-    for cp in waits + locals_:
+        for k in range(1, depth):
+            recv["z", a, k].wait_recv()
+            who = line[k] + x
+            dst = pairs[a][1]
+            send(("x", a, k), at(dst, who, first, direct), at(dst, who, first, direct), (xs, xr), (a, k), partner)
+            spread(a, who, k)
+        if a == 1:
+            open_small(1)
+            open_small(2)
+        for k in range(depth):
+            recv["x", a, k].wait_recv()
+            spread(a, line[k] + 1 - x, depth + k)
+    for b in range(3):
+        dst = small[b][1]
+        size = small[b][0].shape[0]
+        for k in range(1, depth):
+            recv["z", 2 + b, k].wait_recv()
+            who = line[k] + x
+            send(("x", 2 + b, k), block(dst, who, size), block(dst, who, size), (xs, xr), (2 + b, k), partner)
+    for a in range(2):
+        dst = pairs[a][1]
+        for n in range(1, 2 * depth):
+            recv["y", a, n].wait_recv()
+            who = line[n] + x if n < depth else line[n - depth] + 1 - x
+            send(("t", a, n), at(dst, who, back, passed), at(dst, who, back, passed), (ts, tr), (a, n), sibling)
+    for b in range(3):
+        for k in range(depth):
+            recv["x", 2 + b, k].wait_recv()
+    for a in range(2):
+        for n in range(1, 2 * depth):
+            recv["s", a, n].wait_recv()
+            recv["t", a, n].wait_recv()
+    for cp in recv.values():
+        cp.wait_send()
+    for cp in waits:
         cp.wait()
 
 
@@ -174,109 +211,142 @@
         out_shape=outs,
         in_specs=[pl.BlockSpec(memory_space=pltpu.VMEM)] * 5,
         out_specs=[pl.BlockSpec(memory_space=pl.ANY)] * 5,
-        scratch_shapes=[dma((2, sp_count))] * 4 + [dma((2, sp_count, 2))] * 2 + [dma((3, sp_count))] * 2 + [dma((5,))],
+        scratch_shapes=[dma((5, sp_count))] * 4 + [dma((2, sp_count))] * 6 + [dma((5,))],
         compiler_params=pltpu.CompilerParams(collective_id=0, has_side_effects=True),
     )(x, g, info, r, h)
 
 
-def return_kernel(sp_count, p_ref, g_ref, mixed, cols_out, sib, out, got, ybuf, yown,
-                  a_s, a_r, b_s, b_r, c_s, c_r, d_s, d_r, local_sem):
+def return_kernel(sp_count, p_ref, g_ref, mixed, sib, out, ygot, last, got,
+                  a_s, a_r, y_s, y_r, b_s, b_r, c_s, c_r):
     me, side, core, peers, sources, sibling, across = places(sp_count)
     rows, feats = g_ref.shape
-    half = feats // 2
+    half, quarter = feats // 2, feats // 4
     mine = pl.multiple_of(core * half, half)
     theirs = pl.multiple_of((1 - core) * half, half)
+    own = pl.ds(pl.multiple_of(side * quarter, quarter), quarter)
+    other = pl.ds(pl.multiple_of((1 - side) * quarter, quarter), quarter)
     greet(peers[1:] + [sibling, across])
-    order = list(range(1, sp_count)) + [0]
-    first = {}
+    order = list(range(sp_count // 2, 0, -1)) + list(range(sp_count // 2 + 1, sp_count)) + [0]
+    first, second, third = {}, {}, {}
     for k in order:
         at = pl.ds(pl.multiple_of(peers[k][0] * rows, rows), rows)
         first[k] = remote(p_ref.at[at, pl.ds(theirs, half)], sib.at[k], a_s.at[k], a_r.at[k], sibling)
         first[k].start()
-    second = {}
     for k in order:
         at = pl.ds(pl.multiple_of(peers[k][0] * rows, rows), rows)
         first[k].wait_recv()
         total = p_ref[at, pl.ds(mine, half)].astype(jnp.float32) + sib[k].astype(jnp.float32)
         out[k] = total.astype(jnp.bfloat16)
+        second[k] = remote(out.at[k, :, other], ygot.at[k], y_s.at[k], y_r.at[k], across)
+        second[k].start()
+    for k in order:
+        second[k].wait_recv()
+        total = out[k, :, own].astype(jnp.float32) + ygot[k].astype(jnp.float32)
+        last[k] = total.astype(jnp.bfloat16)
         if k:
-            second[k] = remote(out.at[k], got.at[k], b_s.at[k], b_r.at[k], peers[k])
-            second[k].start()
-    total = out[0].astype(jnp.float32)
-    for k in range(1, sp_count):
-        second[k].wait_recv()
+            third[k] = remote(last.at[k], got.at[k], b_s.at[k], b_r.at[k], peers[k])
+            third[k].start()
+    total = last[0].astype(jnp.float32)
+    for k in order[:-1]:
+        third[k].wait_recv()
         total = total + got[k].astype(jnp.float32)
-    yown[...] = total.astype(jnp.bfloat16)
-    cross = remote(yown, ybuf, c_s.at[0], c_r.at[0], across)
-    cross.start()
-    cross.wait()
-    part = pl.ds(mine, half)
-    total = yown[...].astype(jnp.float32) + ybuf[...].astype(jnp.float32)
-    mixed[:, part] = (g_ref[:, part].astype(jnp.float32) + total).astype(jnp.bfloat16)
-    share = remote(mixed.at[:, part], mixed.at[:, part], c_s.at[1], c_r.at[1], sibling)
-    share.start()
-    share.wait()
+    here = pl.ds(pl.multiple_of(core * half + side * quarter, quarter), quarter)
+    there = pl.ds(pl.multiple_of(core * half + (1 - side) * quarter, quarter), quarter)
+    mixed[:, here] = (g_ref[:, here].astype(jnp.float32) + total).astype(jnp.bfloat16)
+    ends = []
+    for n, (cols, who) in enumerate(((here, across), (here, sibling), (there, sibling))):
+        if n == 2:
+            ends[0].wait_recv()
+        cp = remote(mixed.at[:, cols], mixed.at[:, cols], c_s.at[n], c_r.at[n], who)
+        cp.start()
+        ends.append(cp)
+    ends[1].wait_recv()
+    ends[2].wait_recv()
+    for cp in ends + list(first.values()) + list(second.values()) + list(third.values()):
+        cp.wait_send()
+
+
+def return_all(sp_count, partial, g):
+    dma = pltpu.SemaphoreType.DMA
+    rows, feats = g.shape
+    big = pltpu.VMEM((sp_count, rows, feats // 2), jnp.bfloat16)
+    small = pltpu.VMEM((sp_count, rows, feats // 4), jnp.bfloat16)
+    return pl.pallas_call(
+        functools.partial(return_kernel, sp_count),
+        out_shape=jax.ShapeDtypeStruct((rows, feats), jnp.bfloat16),
+        in_specs=[pl.BlockSpec(memory_space=pltpu.VMEM)] * 2,
+        out_specs=pl.BlockSpec(memory_space=pltpu.VMEM),
+        scratch_shapes=[big, big, small, small, small] + [dma((sp_count,))] * 6 + [dma((3,))] * 2,
+        compiler_params=pltpu.CompilerParams(collective_id=1, has_side_effects=True),
+    )(partial, g)
+
+
+def carry_kernel(sp_count, mixed, decay_ref, up_ref, dstate, cols_out, block, got, s, r, d_s, d_r, local_sem):
+    me, side, core, peers, sources, sibling, across = places(sp_count)
+    rows, feats = mixed.shape
     width = feats // sp_count
+    greet(peers[1:])
     own = pl.ds(pl.multiple_of(me * rows, rows), rows)
-    last = []
+    moved = []
     for k in range(1, sp_count):
         cols = pl.ds(pl.multiple_of(peers[k][0] * width, width), width)
         cp = remote(mixed.at[:, cols], cols_out.at[own, :], d_s.at[k], d_r.at[k], peers[k])
         cp.start()
-        last.append(cp)
-    here = pltpu.make_async_copy(mixed.at[:, pl.ds(pl.multiple_of(me * width, width), width)], cols_out.at[own, :], local_sem)
+        moved.append(cp)
+    here = pltpu.make_async_copy(
+        mixed.at[:, pl.ds(pl.multiple_of(me * width, width), width)], cols_out.at[own, :], local_sem
+    )
     here.start()
+    row = lax.broadcasted_iota(jnp.int32, up_ref.shape, 0)
+    decay = decay_ref[...]
+    prod = jnp.where(row < rows - 1, pltpu.roll(decay, rows - 1, 0), 1.0)
+    part = up_ref[...]
+    step = 1
+    while step < rows:
+        keep = row < rows - step
+        later = jnp.where(keep, pltpu.roll(part, rows - step, 0), 0.0)
+        after = jnp.where(keep, pltpu.roll(prod, rows - step, 0), 1.0)
+        part = part + prod * later
+        prod = prod * after
+        step *= 2
+    block[...] = jnp.zeros_like(block)
+    got[me] = jnp.zeros(block.shape, jnp.float32)
+    block[0:1] = decay[0:1] * prod[0:1]
+    block[1:2] = decay[0:1] * part[0:1]
+    copies = []
+    for k in range(1, sp_count):
+        cp = remote(block, got.at[me], s.at[k], r.at[k], peers[k])
+        cp.start()
+        copies.append(cp)
+    for cp in copies:
+        cp.wait()
+    incoming = jnp.zeros((1, up_ref.shape[1]), jnp.float32)
+    for source in range(sp_count - 1, 0, -1):
+        value = got[source]
+        incoming = jnp.where(source > me, value[1:2] + value[0:1] * incoming, incoming)
+    dstate[...] = part + prod * incoming
     here.wait()
-    for cp in last:
+    for cp in moved:
         cp.wait()
-    for k in order:
-        first[k].wait_send()
-    for k in range(1, sp_count):
-        second[k].wait_send()
-
-
-def return_all(sp_count, partial, g):
+
+
+def carry_all(sp_count, mixed, decay, upstream):
     dma = pltpu.SemaphoreType.DMA
-    rows, feats = g.shape
-    half = feats // 2
-    big = pltpu.VMEM((sp_count, rows, half), jnp.bfloat16)
-    one = pltpu.VMEM((rows, half), jnp.bfloat16)
+    rows, feats = mixed.shape
+    block = (8, upstream.shape[1])
     return pl.pallas_call(
-        functools.partial(return_kernel, sp_count),
+        functools.partial(carry_kernel, sp_count),
         out_shape=[
-            jax.ShapeDtypeStruct((rows, feats), jnp.bfloat16),
+            jax.ShapeDtypeStruct(upstream.shape, jnp.float32),
             jax.ShapeDtypeStruct((rows * sp_count, feats // sp_count), jnp.bfloat16),
         ],
-        in_specs=[pl.BlockSpec(memory_space=pltpu.VMEM)] * 2,
+        in_specs=[pl.BlockSpec(memory_space=pltpu.VMEM)] * 3,
         out_specs=[pl.BlockSpec(memory_space=pltpu.VMEM)] * 2,
-        scratch_shapes=[big, big, big, one, one] + [dma((sp_count,))] * 4 + [dma((2,))] * 2 + [dma((sp_count,))] * 2 + [dma],
-        compiler_params=pltpu.CompilerParams(collective_id=1, has_side_effects=True),
-    )(partial, g)
-
-
-def carry_kernel(sp_count, c_ref, got, s, r):
-    me, side, core, peers, sources, sibling, across = places(sp_count)
-    greet(peers[1:])
-    copies = []
-    for k in range(1, sp_count):
-        cp = remote(c_ref, got.at[me], s.at[k], r.at[k], peers[k])
-        cp.start()
-        copies.append(cp)
-    got[me] = c_ref[...]
-    for cp in copies:
-        cp.wait()
-
-
-def carry_all(sp_count, block):
-    dma = pltpu.SemaphoreType.DMA
-    return pl.pallas_call(
-        functools.partial(carry_kernel, sp_count),
-        out_shape=jax.ShapeDtypeStruct((sp_count,) + block.shape, block.dtype),
-        in_specs=[pl.BlockSpec(memory_space=pltpu.VMEM)],
-        out_specs=pl.BlockSpec(memory_space=pltpu.VMEM),
-        scratch_shapes=[dma((sp_count,))] * 2,
+        scratch_shapes=[pltpu.VMEM(block, jnp.float32), pltpu.VMEM((sp_count,) + block, jnp.float32)]
+        + [dma((sp_count,))] * 4
+        + [dma],
         compiler_params=pltpu.CompilerParams(collective_id=2, has_side_effects=True),
-    )(block)
+    )(mixed, decay, upstream)
 
 
 def local(
@@ -496,7 +566,7 @@
         specialist_widen_maps[0],
         specialist_shrink_maps[0],
     )
-    mixed_grad, mixed_cols = return_all(
+    mixed_grad = return_all(
         sp_count, token_part.astype(jnp.bfloat16), result_cotangent_values
     )
     col_count = memory_readout_map.shape[1]
@@ -522,23 +592,7 @@
     spare_room = -jnp.expm1(2.0 * log_fading_factor)
     in_scale = jnp.sqrt(jnp.maximum(spare_room, 0.01))
     drive = in_scale * inp_open * xin
-    coeff = jnp.concatenate([decay_mult[1:], jnp.ones((1, col_count), jnp.float32)], axis=0)
-    prod_after, local_part = lax.associative_scan(compose, (coeff, upstream), reverse=True, axis=0)
-    alpha_part = decay_mult[0] * local_part[0]
-    beta_part = decay_mult[0] * prod_after[0]
-    gathered = carry_all(
-        sp_count,
-        jnp.concatenate(
-            [beta_part[None], alpha_part[None], jnp.zeros((6, col_count), jnp.float32)], axis=0
-        ),
-    )
-    place = lax.axis_index("sp")
-    incoming = jnp.zeros((col_count,), jnp.float32)
-    for source in range(sp_count - 1, 0, -1):
-        incoming = jnp.where(
-            source > place, gathered[source, 1] + gathered[source, 0] * incoming, incoming
-        )
-    dstate = local_part + prod_after * incoming[None, :]
+    dstate, mixed_cols = carry_all(sp_count, mixed_grad, decay_mult, upstream)
     scale_slope = jnp.where(spare_room > 0.01, -decay_mult * decay_mult / in_scale, 0.0)
     log_grad = dstate * (
         memory_hidden_values.astype(jnp.float32) - drive + scale_slope * inp_open * xin

time: 288 us -> 203 us (0.70)
  Pallas kernels: 221 us -> 155 us
  local copies, waits for them, and re-layouts: 12.4 us -> 1.09 us
  other arithmetic: 13.6 us -> 5.37 us
    pallas_call x1, Pallas kernels: 127 us -> 90.4 us  [gather_all(): pl.pallas_call(functools.partial(gather_kernel, sp_count), out_shape=outs...]
    pallas_call x2, Pallas kernels: 94.3 us -> 65 us  [the longest x1 44.2 us: return_all(): pl.pallas_call(functools.partial(return_kernel, sp_count), out_shape=jax....]
    slice x50 -> x0, local copies, waits for them, and re-layouts: 4.99 us -> none  [the longest x49 4.96 us: direct(): lax.associative_scan(compose, (coeff, upstream), reverse=True, axis=0)]
    mul x13 -> x0, other arithmetic: 4.59 us -> none  [the longest x12 3.86 us: compose(): lower_map[0] * upper_map[0]]
    rev x2 -> x0, local copies, waits for them, and re-layouts: 4.3 us -> none  [direct(): lax.associative_scan(compose, (coeff, upstream), reverse=True, axis=0)]
where the time goes in v2:
time: 203 us; the launch traced here: 202 us
  Pallas kernels  155 us (76%)
  matrix products  39.5 us (19%)
  other arithmetic  5.37 us (3%)
    pallas_call x1, Pallas kernels, gather_all(): pl.pallas_call(functools.partial(gather_kernel, sp_count), out_shape=outs...  90.4 us
    pallas_call x1, Pallas kernels, return_all(): pl.pallas_call(functools.partial(return_kernel, sp_count), out_shape=jax....  44.2 us
    pallas_call x1, Pallas kernels, carry_all(): pl.pallas_call(functools.partial(carry_kernel, sp_count), out_shape=[jax....  20.8 us
    dot_general x1, matrix products, expert_backward(): jnp.einsum('rd,fd->rf', grads_in, down_weight, preferred_element_type=jnp...  6.64 us
    dot_general x1, matrix products, expert_backward(): jnp.dot(inputs, gate_weight, preferred_element_type=jnp.float32)  5.66 us
    dot_general x1, matrix products, expert_backward(): jnp.einsum('rf,df->rd', up_grad, up_weight, preferred_element_type=jnp.fl...  4.54 us

profile of v2, /device:TPU:0, one launch (start us, length us, event | category | flops | bytes accessed | tf_op | source)
XLA Modules:
  0.0 202.2 jit_solution(6632460530383640976)
XLA Ops:
  0.6 0.0 copy-start
  0.6 0.8 convert_bitcast_fusion
  1.5 0.1 pad.2.clone
  1.5 1.3 maximum_maximum_fusion.info_ref
  2.9 90.4 %shard_map.173 = (bf16[1024,2048]{1,0:T(8,128)(2,1)}, bf16[1024,2048]{1,0:T(8,128)(2,1)}, f32[64,128]{1,0:T(8,128)}, bf16[2048,512]{1,0:T(8,128)(2,1)}, bf16[1024,512]{1,0:T(8,128)(2,1)}) custom-call(bf16[128,2048]{1,0:T(8,128)(2,1)} %x_ref.1, bf16[128,2048]{1,0:T(8,128)(2,1)} %g_ref.3, f32[8,128]{1,0:T(8,128)} %maximum_maximum_fusion.info_ref, ...), custom_call_target="tpu_custom_call" | custom-call | tf_op jit(solution)/shard_map/pallas_call | solution.py:209
  93.3 0.0 copy-done
  93.3 0.0 copy-start.12
  93.3 0.0 copy-start.14
  93.4 5.7 %fusion.5 = f32[1024,448]{0,1:T(8,128)} fusion(bf16[1024,2048]{1,0:T(8,128)(2,1)} %get-tuple-element.12, bf16[1,2048,448]{1,2,0:T(8,128)(2,1)S(1)} %copy-done), kind=kOutput, calls=%fused_computation.10 | convolution fusion | flops 1879048192 | bytes 7864320 | tf_op jit(solution)/shard_map/dot_general | solution.py:43
  99.0 0.0 copy-done.12
  99.0 0.0 copy-done.14
  99.0 0.0 copy-start.8
  99.0 3.3 %fusion.8 = f32[1024,448]{0,1:T(8,128)} fusion(bf16[1024,2048]{1,0:T(8,128)(2,1)S(1)} %copy-done.12, bf16[1,2048,448]{1,2,0:T(8,128)(2,1)S(1)} %copy-done.14), kind=kOutput, calls=%fused_computation.13 | convolution fusion | flops 1879048192 | bytes 7864320 | tf_op jit(solution)/shard_map/dot_general | solution.py:44
  102.4 0.0 copy-done.8
  102.4 0.0 copy-start.13
  102.4 6.6 %multiply_convert_fusion.2 = (bf16[1024,448]{0,1:T(8,128)(2,1)S(1)}, bf16[1024,448]{0,1:T(8,128)(2,1)S(1)}) fusion(f32[1024,448]{0,1:T(8,128)} %fusion.5, f32[1024,448]{0,1:T(8,128)} %fusion.8, bf16[1,448,2048]{2,1,0:T(8,128)(2,1)} %param.20, bf16[1024,2048]{1,0:T(8,128)(2,1)} %get-tuple-element.14, f32[1024]{0:T(1024)S(1)} %bitcast.79), kind=kOutput, calls=%fused_computation.18 | convolution fusion | flops 1891303424 | bytes 11538432 | tf_op jit(solution)/shard_map/rd,fd->rf/dot_general | solution.py:50
  109.0 0.0 copy-done.13
  109.1 3.3 %fusion.1 = bf16[1,2048,448]{1,2,0:T(8,128)(2,1)} fusion(bf16[1024,448]{0,1:T(8,128)(2,1)S(1)} %get-tuple-element.20, bf16[1024,2048]{1,0:T(8,128)(2,1)S(1)} %copy-done.13), kind=kOutput, calls=%fused_computation.6 | convolution fusion | flops 1879965696 | bytes 6946816 | tf_op jit(solution)/shard_map/rd,rf->df/dot_general | solution.py:53
  112.4 0.0 copy-start.11
  112.4 0.0 copy-start.16
  112.4 0.0 copy-start.17
  112.4 3.3 %fusion.2 = bf16[1,2048,448]{1,2,0:T(8,128)(2,1)} fusion(bf16[1024,448]{0,1:T(8,128)(2,1)S(1)} %get-tuple-element.19, bf16[1024,2048]{1,0:T(8,128)(2,1)S(1)} %copy-done.13), kind=kOutput, calls=%fused_computation.7 | convolution fusion | flops 1879965696 | bytes 6946816 | tf_op jit(solution)/shard_map/rd,rf->df/dot_general | solution.py:56
  115.7 0.0 copy-done.11
  115.7 0.0 copy-done.16
  115.7 0.4 copy-done.17
  116.2 3.8 %fusion = bf16[1,448,2048]{2,1,0:T(8,128)(2,1)} fusion(bf16[1024,2048]{1,0:T(8,128)(2,1)S(1)} %copy-done.11, f32[1024]{0:T(1024)S(1)} %bitcast.80, f32[1024,448]{0,1:T(8,128)S(1)} %copy-done.17, f32[1024,448]{0,1:T(8,128)S(1)} %copy-done.16), kind=kOutput, calls=%fused_computation.5 | convolution fusion | flops 1889009664 | bytes 9703424 | tf_op jit(solution)/shard_map/rf,rd->fd/dot_general | solution.py:47
  119.9 0.0 copy-start.15
  119.9 2.4 %fusion.3 = f32[1024,2048]{1,0:T(8,128)S(1)} fusion(bf16[1024,448]{0,1:T(8,128)(2,1)S(1)} %get-tuple-element.20, bf16[1,2048,448]{1,2,0:T(8,128)(2,1)S(1)} %copy-done), kind=kOutput, calls=%fused_computation.8 | convolution fusion | flops 1879048192 | bytes 11141120 | tf_op jit(solution)/shard_map/rf,df->rd/dot_general | solution.py:59
  122.3 0.0 copy-done.15
  122.3 4.5 %add_convert_fusion.p_ref = bf16[1024,2048]{1,0:T(8,128)(2,1)} fusion(f32[1024,2048]{1,0:T(8,128)S(1)} %fusion.3, bf16[1024,448]{0,1:T(8,128)(2,1)S(1)} %get-tuple-element.19, bf16[1,2048,448]{1,2,0:T(8,128)(2,1)S(1)} %copy-done.15), kind=kOutput, calls=%fused_computation | convolution fusion | flops 1883242496 | bytes 15335424 | tf_op jit(solution)/shard_map/rf,df->rd/dot_general | solution.py:60
  126.9 0.0 copy-start.5
  126.9 0.0 copy-start.6
  126.9 44.2 %shard_map.174.mixed = bf16[128,2048]{1,0:T(8,128)(2,1)} custom-call(bf16[1024,2048]{1,0:T(8,128)(2,1)} %add_convert_fusion.p_ref, bf16[128,2048]{1,0:T(8,128)(2,1)} %g_ref.3), custom_call_target="tpu_custom_call" | custom-call | tf_op jit(solution)/shard_map/pallas_call | solution.py:274
  171.1 0.0 copy-start.10
  171.1 0.0 copy-start.9
  171.1 0.0 copy-start.1
  171.1 0.0 copy-done.5
  171.1 0.0 copy-done.6
  171.2 0.3 fusion.18
  171.5 0.1 copy.31
  171.6 0.2 copy-done.10
  171.8 0.0 copy-done.9
  171.8 0.8 fusion.33.decay_ref
  172.6 0.0 copy-done.1
  172.6 2.7 %fusion.45.up_ref = f32[128,512]{1,0:T(8,128)} fusion(bf16[128,2048]{1,0:T(8,128)(2,1)S(1)} %copy-done.1, bf16[2048,512]{1,0:T(8,128)(2,1)} %get-tuple-element.15), kind=kOutput, calls=%fused_computation.70 | convolution fusion | flops 268435456 | bytes 2883584 | tf_op jit(solution)/shard_map/dot_general | solution.py:573
  175.3 0.0 copy-start.4
  175.4 0.0 copy-start.7
  175.4 20.8 %shard_map.175 = (f32[128,512]{1,0:T(8,128)}, bf16[1024,256]{1,0:T(8,128)(2,1)}) custom-call(bf16[128,2048]{1,0:T(8,128)(2,1)} %shard_map.174.mixed, f32[128,512]{1,0:T(8,128)} %fusion.33.decay_ref, f32[128,512]{1,0:T(8,128)} %fusion.45.up_ref), custom_call_target="tpu_custom_call" | custom-call | tf_op jit(solution)/shard_map/pallas_call | solution.py:337
  196.2 0.0 copy-start.2
  196.2 0.0 copy-start.3
  196.2 2.7 %fusion.46 = f32[256,512]{1,0:T(8,128)} fusion(bf16[1024,256]{1,0:T(8,128)(2,1)} %get-tuple-element.16, bf16[1024,512]{1,0:T(8,128)(2,1)} %get-tuple-element.17), kind=kOutput, calls=%fused_computation.71 | convolution fusion | flops 268435456 | bytes 2097152 | tf_op jit(solution)/shard_map/tr,tc->rc/dot_general | solution.py:624
  198.9 0.0 copy-done.4
  198.9 0.0 copy-done.7
  198.9 0.3 fusion.15
  199.2 0.1 copy.32
  199.3 0.0 copy-done.2
  199.3 0.0 copy-done.3
  199.3 1.4 fusion.26
  200.7 0.2 convolution_bitcast_fusion
  201.0 0.2 convolution_bitcast_fusion.1
  201.2 1.0 add_add_fusion
  (5 shorter events, 0.1 us)
Async XLA Ops:
  0.6 92.7 %copy-start = (bf16[1,2048,448]{1,2,0:T(8,128)(2,1)S(1)}, bf16[1,2048,448]{1,2,0:T(8,128)(2,1)}, u32[]{:S(2)}) copy-start(bf16[1,2048,448]{1,2,0:T(8,128)(2,1)} %param.18) | copy-start | bytes 5505028
  93.3 5.7 %copy-start.12 = (bf16[1024,2048]{1,0:T(8,128)(2,1)S(1)}, bf16[1024,2048]{1,0:T(8,128)(2,1)}, u32[]{:S(2)}) copy-start(bf16[1024,2048]{1,0:T(8,128)(2,1)} %get-tuple-element.12) | copy-start | bytes 12582916
  93.3 5.7 %copy-start.14 = (bf16[1,2048,448]{1,2,0:T(8,128)(2,1)S(1)}, bf16[1,2048,448]{1,2,0:T(8,128)(2,1)}, u32[]{:S(2)}) copy-start(bf16[1,2048,448]{1,2,0:T(8,128)(2,1)} %param.19) | copy-start | bytes 5505028
  99.0 3.3 %copy-start.8 = (f32[64,128]{1,0:T(8,128)S(1)}, f32[64,128]{1,0:T(8,128)}, u32[]{:S(2)}) copy-start(f32[64,128]{1,0:T(8,128)} %get-tuple-element.13) | copy-start | bytes 98308
  102.4 6.7 %copy-start.13 = (bf16[1024,2048]{1,0:T(8,128)(2,1)S(1)}, bf16[1024,2048]{1,0:T(8,128)(2,1)}, u32[]{:S(2)}) copy-start(bf16[1024,2048]{1,0:T(8,128)(2,1)} %get-tuple-element.12) | copy-start | bytes 12582916
  112.4 3.3 %copy-start.11 = (bf16[1024,2048]{1,0:T(8,128)(2,1)S(1)}, bf16[1024,2048]{1,0:T(8,128)(2,1)}, u32[]{:S(2)}) copy-start(bf16[1024,2048]{1,0:T(8,128)(2,1)} %get-tuple-element.14) | copy-start | bytes 12582916
  112.4 3.3 %copy-start.16 = (f32[1024,448]{0,1:T(8,128)S(1)}, f32[1024,448]{0,1:T(8,128)}, u32[]{:S(2)}) copy-start(f32[1024,448]{0,1:T(8,128)} %fusion.5) | copy-start | bytes 5505028
  112.4 3.8 %copy-start.17 = (f32[1024,448]{0,1:T(8,128)S(1)}, f32[1024,448]{0,1:T(8,128)}, u32[]{:S(2)}) copy-start(f32[1024,448]{0,1:T(8,128)} %fusion.8) | copy-start | bytes 5505028
  119.9 2.4 %copy-start.15 = (bf16[1,2048,448]{1,2,0:T(8,128)(2,1)S(1)}, bf16[1,2048,448]{1,2,0:T(8,128)(2,1)}, u32[]{:S(2)}) copy-start(bf16[1,2048,448]{1,2,0:T(8,128)(2,1)} %param.19) | copy-start | bytes 5505028
  126.9 44.2 %copy-start.5 = (bf16[2,256,256]{2,1,0:T(8,128)(2,1)S(1)}, bf16[2,256,256]{2,1,0:T(8,128)(2,1)}, u32[]{:S(2)}) copy-start(bf16[2,256,256]{2,1,0:T(8,128)(2,1)} %param.26) | copy-start | bytes 786436
  126.9 44.3 %copy-start.6 = (bf16[128,512]{1,0:T(8,128)(2,1)S(1)}, bf16[128,512]{1,0:T(8,128)(2,1)}, u32[]{:S(2)}) copy-start(bf16[128,512]{1,0:T(8,128)(2,1)} %param.22) | copy-start | bytes 393220
  171.1 0.7 copy-start.10
  171.1 0.7 copy-start.9
  171.1 1.5 copy-start.1
  175.3 23.5 %copy-start.4 = (bf16[2,256,256]{2,1,0:T(8,128)(2,1)S(1)}, bf16[2,256,256]{2,1,0:T(8,128)(2,1)}, u32[]{:S(2)}) copy-start(bf16[2,256,256]{2,1,0:T(8,128)(2,1)} %param.27) | copy-start | bytes 786436
  175.4 23.5 %copy-start.7 = (bf16[128,512]{1,0:T(8,128)(2,1)S(1)}, bf16[128,512]{1,0:T(8,128)(2,1)}, u32[]{:S(2)}) copy-start(bf16[128,512]{1,0:T(8,128)(2,1)} %param.22) | copy-start | bytes 393220
  196.2 3.1 %copy-start.2 = (f32[128,512]{1,0:T(8,128)S(1)}, f32[128,512]{1,0:T(8,128)}, u32[]{:S(2)}) copy-start(f32[128,512]{1,0:T(8,128)} %get-tuple-element.18) | copy-start | bytes 786436
  196.2 3.1 %copy-start.3 = (bf16[128,512]{1,0:T(8,128)(2,1)S(1)}, bf16[128,512]{1,0:T(8,128)(2,1)}, u32[]{:S(2)}) copy-start(bf16[128,512]{1,0:T(8,128)(2,1)} %h_ref.1) | copy-start | bytes 393220

commit v3 on v2

--- a/solution.py
+++ b/solution.py
@@ -164,6 +164,8 @@
     open_pair(0)
     open_small(0)
     open_pair(1)
+    open_small(1)
+    open_small(2)
     for a in range(2):
         for k in range(1, depth):
             recv["z", a, k].wait_recv()
@@ -171,9 +173,6 @@
             dst = pairs[a][1]
             send(("x", a, k), at(dst, who, first, direct), at(dst, who, first, direct), (xs, xr), (a, k), partner)
             spread(a, who, k)
-        if a == 1:
-            open_small(1)
-            open_small(2)
         for k in range(depth):
             recv["x", a, k].wait_recv()
             spread(a, line[k] + 1 - x, depth + k)

time: 203 us -> 203 us (level)
    pallas_call x1, Pallas kernels: 44.2 us -> 46.8 us  [return_all(): pl.pallas_call(functools.partial(return_kernel, sp_count), out_shape=jax....]
    pallas_call x1, Pallas kernels: 90.4 us -> 87.8 us  [gather_all(): pl.pallas_call(functools.partial(gather_kernel, sp_count), out_shape=outs...]
where the time goes in v3:
time: 203 us; the launch traced here: 202 us
  Pallas kernels  155 us (76%)
  matrix products  39.5 us (19%)
  other arithmetic  5.37 us (3%)
    pallas_call x1, Pallas kernels, gather_all(): pl.pallas_call(functools.partial(gather_kernel, sp_count), out_shape=outs...  87.8 us
    pallas_call x1, Pallas kernels, return_all(): pl.pallas_call(functools.partial(return_kernel, sp_count), out_shape=jax....  46.8 us
    pallas_call x1, Pallas kernels, carry_all(): pl.pallas_call(functools.partial(carry_kernel, sp_count), out_shape=[jax....  20.8 us
    dot_general x1, matrix products, expert_backward(): jnp.einsum('rd,fd->rf', grads_in, down_weight, preferred_element_type=jnp...  6.64 us
    dot_general x1, matrix products, expert_backward(): jnp.dot(inputs, gate_weight, preferred_element_type=jnp.float32)  5.66 us
    dot_general x1, matrix products, expert_backward(): jnp.einsum('rf,df->rd', up_grad, up_weight, preferred_element_type=jnp.fl...  4.54 us

profile of v3, /device:TPU:0, one launch (start us, length us, event | category | flops | bytes accessed | tf_op | source)
XLA Modules:
  0.0 202.3 jit_solution(15510889130368707027)
XLA Ops:
  0.6 0.0 copy-start
  0.6 0.8 convert_bitcast_fusion
  1.5 0.1 pad.2.clone
  1.5 1.3 maximum_maximum_fusion.info_ref
  2.9 87.8 %shard_map.173 = (bf16[1024,2048]{1,0:T(8,128)(2,1)}, bf16[1024,2048]{1,0:T(8,128)(2,1)}, f32[64,128]{1,0:T(8,128)}, bf16[2048,512]{1,0:T(8,128)(2,1)}, bf16[1024,512]{1,0:T(8,128)(2,1)}) custom-call(bf16[128,2048]{1,0:T(8,128)(2,1)} %x_ref.1, bf16[128,2048]{1,0:T(8,128)(2,1)} %g_ref.3, f32[8,128]{1,0:T(8,128)} %maximum_maximum_fusion.info_ref, ...), custom_call_target="tpu_custom_call" | custom-call | tf_op jit(solution)/shard_map/pallas_call | solution.py:208
  90.7 0.0 copy-done
  90.7 0.0 copy-start.12
  90.7 0.0 copy-start.14
  90.8 5.7 %fusion.5 = f32[1024,448]{0,1:T(8,128)} fusion(bf16[1024,2048]{1,0:T(8,128)(2,1)} %get-tuple-element.12, bf16[1,2048,448]{1,2,0:T(8,128)(2,1)S(1)} %copy-done), kind=kOutput, calls=%fused_computation.10 | convolution fusion | flops 1879048192 | bytes 7864320 | tf_op jit(solution)/shard_map/dot_general | solution.py:43
  96.4 0.0 copy-done.12
  96.4 0.0 copy-done.14
  96.4 0.0 copy-start.8
  96.4 3.3 %fusion.8 = f32[1024,448]{0,1:T(8,128)} fusion(bf16[1024,2048]{1,0:T(8,128)(2,1)S(1)} %copy-done.12, bf16[1,2048,448]{1,2,0:T(8,128)(2,1)S(1)} %copy-done.14), kind=kOutput, calls=%fused_computation.13 | convolution fusion | flops 1879048192 | bytes 7864320 | tf_op jit(solution)/shard_map/dot_general | solution.py:44
  99.8 0.0 copy-done.8
  99.8 0.0 copy-start.13
  99.8 6.6 %multiply_convert_fusion.2 = (bf16[1024,448]{0,1:T(8,128)(2,1)S(1)}, bf16[1024,448]{0,1:T(8,128)(2,1)S(1)}) fusion(f32[1024,448]{0,1:T(8,128)} %fusion.5, f32[1024,448]{0,1:T(8,128)} %fusion.8, bf16[1,448,2048]{2,1,0:T(8,128)(2,1)} %param.20, bf16[1024,2048]{1,0:T(8,128)(2,1)} %get-tuple-element.14, f32[1024]{0:T(1024)S(1)} %bitcast.79), kind=kOutput, calls=%fused_computation.18 | convolution fusion | flops 1891303424 | bytes 11538432 | tf_op jit(solution)/shard_map/rd,fd->rf/dot_general | solution.py:50
  106.5 0.0 copy-done.13
  106.5 3.3 %fusion.1 = bf16[1,2048,448]{1,2,0:T(8,128)(2,1)} fusion(bf16[1024,448]{0,1:T(8,128)(2,1)S(1)} %get-tuple-element.20, bf16[1024,2048]{1,0:T(8,128)(2,1)S(1)} %copy-done.13), kind=kOutput, calls=%fused_computation.6 | convolution fusion | flops 1879965696 | bytes 6946816 | tf_op jit(solution)/shard_map/rd,rf->df/dot_general | solution.py:53
  109.8 0.0 copy-start.11
  109.8 0.0 copy-start.16
  109.8 0.0 copy-start.17
  109.8 3.3 %fusion.2 = bf16[1,2048,448]{1,2,0:T(8,128)(2,1)} fusion(bf16[1024,448]{0,1:T(8,128)(2,1)S(1)} %get-tuple-element.19, bf16[1024,2048]{1,0:T(8,128)(2,1)S(1)} %copy-done.13), kind=kOutput, calls=%fused_computation.7 | convolution fusion | flops 1879965696 | bytes 6946816 | tf_op jit(solution)/shard_map/rd,rf->df/dot_general | solution.py:56
  113.1 0.0 copy-done.11
  113.1 0.0 copy-done.16
  113.1 0.4 copy-done.17
  113.6 3.8 %fusion = bf16[1,448,2048]{2,1,0:T(8,128)(2,1)} fusion(bf16[1024,2048]{1,0:T(8,128)(2,1)S(1)} %copy-done.11, f32[1024]{0:T(1024)S(1)} %bitcast.80, f32[1024,448]{0,1:T(8,128)S(1)} %copy-done.17, f32[1024,448]{0,1:T(8,128)S(1)} %copy-done.16), kind=kOutput, calls=%fused_computation.5 | convolution fusion | flops 1889009664 | bytes 9703424 | tf_op jit(solution)/shard_map/rf,rd->fd/dot_general | solution.py:47
  117.3 0.0 copy-start.15
  117.3 2.4 %fusion.3 = f32[1024,2048]{1,0:T(8,128)S(1)} fusion(bf16[1024,448]{0,1:T(8,128)(2,1)S(1)} %get-tuple-element.20, bf16[1,2048,448]{1,2,0:T(8,128)(2,1)S(1)} %copy-done), kind=kOutput, calls=%fused_computation.8 | convolution fusion | flops 1879048192 | bytes 11141120 | tf_op jit(solution)/shard_map/rf,df->rd/dot_general | solution.py:59
  119.8 0.0 copy-done.15
  119.8 4.5 %add_convert_fusion.p_ref = bf16[1024,2048]{1,0:T(8,128)(2,1)} fusion(f32[1024,2048]{1,0:T(8,128)S(1)} %fusion.3, bf16[1024,448]{0,1:T(8,128)(2,1)S(1)} %get-tuple-element.19, bf16[1,2048,448]{1,2,0:T(8,128)(2,1)S(1)} %copy-done.15), kind=kOutput, calls=%fused_computation | convolution fusion | flops 1883242496 | bytes 15335424 | tf_op jit(solution)/shard_map/rf,df->rd/dot_general | solution.py:60
  124.3 0.0 copy-start.5
  124.3 0.0 copy-start.6
  124.3 46.8 %shard_map.174.mixed = bf16[128,2048]{1,0:T(8,128)(2,1)} custom-call(bf16[1024,2048]{1,0:T(8,128)(2,1)} %add_convert_fusion.p_ref, bf16[128,2048]{1,0:T(8,128)(2,1)} %g_ref.3), custom_call_target="tpu_custom_call" | custom-call | tf_op jit(solution)/shard_map/pallas_call | solution.py:273
  171.1 0.0 copy-start.10
  171.1 0.0 copy-start.9
  171.2 0.0 copy-start.1
  171.2 0.0 copy-done.5
  171.2 0.0 copy-done.6
  171.2 0.3 fusion.18
  171.5 0.1 copy.31
  171.6 0.2 copy-done.10
  171.8 0.0 copy-done.9
  171.8 0.8 fusion.33.decay_ref
  172.6 0.0 copy-done.1
  172.6 2.8 %fusion.45.up_ref = f32[128,512]{1,0:T(8,128)} fusion(bf16[128,2048]{1,0:T(8,128)(2,1)S(1)} %copy-done.1, bf16[2048,512]{1,0:T(8,128)(2,1)} %get-tuple-element.15), kind=kOutput, calls=%fused_computation.70 | convolution fusion | flops 268435456 | bytes 2883584 | tf_op jit(solution)/shard_map/dot_general | solution.py:572
  175.4 0.0 copy-start.4
  175.4 0.0 copy-start.7
  175.4 20.8 %shard_map.175 = (f32[128,512]{1,0:T(8,128)}, bf16[1024,256]{1,0:T(8,128)(2,1)}) custom-call(bf16[128,2048]{1,0:T(8,128)(2,1)} %shard_map.174.mixed, f32[128,512]{1,0:T(8,128)} %fusion.33.decay_ref, f32[128,512]{1,0:T(8,128)} %fusion.45.up_ref), custom_call_target="tpu_custom_call" | custom-call | tf_op jit(solution)/shard_map/pallas_call | solution.py:336
  196.2 0.0 copy-start.2
  196.2 0.0 copy-start.3
  196.2 2.7 %fusion.46 = f32[256,512]{1,0:T(8,128)} fusion(bf16[1024,256]{1,0:T(8,128)(2,1)} %get-tuple-element.16, bf16[1024,512]{1,0:T(8,128)(2,1)} %get-tuple-element.17), kind=kOutput, calls=%fused_computation.71 | convolution fusion | flops 268435456 | bytes 2097152 | tf_op jit(solution)/shard_map/tr,tc->rc/dot_general | solution.py:623
  198.9 0.0 copy-done.4
  198.9 0.0 copy-done.7
  198.9 0.3 fusion.15
  199.2 0.1 copy.32
  199.3 0.0 copy-done.2
  199.4 0.0 copy-done.3
  199.4 1.4 fusion.26
  200.8 0.2 convolution_bitcast_fusion
  201.0 0.2 convolution_bitcast_fusion.1
  201.3 1.0 add_add_fusion
  (5 shorter events, 0.1 us)
Async XLA Ops:
  0.6 90.1 %copy-start = (bf16[1,2048,448]{1,2,0:T(8,128)(2,1)S(1)}, bf16[1,2048,448]{1,2,0:T(8,128)(2,1)}, u32[]{:S(2)}) copy-start(bf16[1,2048,448]{1,2,0:T(8,128)(2,1)} %param.18) | copy-start | bytes 5505028
  90.7 5.7 %copy-start.12 = (bf16[1024,2048]{1,0:T(8,128)(2,1)S(1)}, bf16[1024,2048]{1,0:T(8,128)(2,1)}, u32[]{:S(2)}) copy-start(bf16[1024,2048]{1,0:T(8,128)(2,1)} %get-tuple-element.12) | copy-start | bytes 12582916
  90.7 5.7 %copy-start.14 = (bf16[1,2048,448]{1,2,0:T(8,128)(2,1)S(1)}, bf16[1,2048,448]{1,2,0:T(8,128)(2,1)}, u32[]{:S(2)}) copy-start(bf16[1,2048,448]{1,2,0:T(8,128)(2,1)} %param.19) | copy-start | bytes 5505028
  96.4 3.3 %copy-start.8 = (f32[64,128]{1,0:T(8,128)S(1)}, f32[64,128]{1,0:T(8,128)}, u32[]{:S(2)}) copy-start(f32[64,128]{1,0:T(8,128)} %get-tuple-element.13) | copy-start | bytes 98308
  99.8 6.7 %copy-start.13 = (bf16[1024,2048]{1,0:T(8,128)(2,1)S(1)}, bf16[1024,2048]{1,0:T(8,128)(2,1)}, u32[]{:S(2)}) copy-start(bf16[1024,2048]{1,0:T(8,128)(2,1)} %get-tuple-element.12) | copy-start | bytes 12582916
  109.8 3.3 %copy-start.11 = (bf16[1024,2048]{1,0:T(8,128)(2,1)S(1)}, bf16[1024,2048]{1,0:T(8,128)(2,1)}, u32[]{:S(2)}) copy-start(bf16[1024,2048]{1,0:T(8,128)(2,1)} %get-tuple-element.14) | copy-start | bytes 12582916
  109.8 3.3 %copy-start.16 = (f32[1024,448]{0,1:T(8,128)S(1)}, f32[1024,448]{0,1:T(8,128)}, u32[]{:S(2)}) copy-start(f32[1024,448]{0,1:T(8,128)} %fusion.5) | copy-start | bytes 5505028
  109.8 3.8 %copy-start.17 = (f32[1024,448]{0,1:T(8,128)S(1)}, f32[1024,448]{0,1:T(8,128)}, u32[]{:S(2)}) copy-start(f32[1024,448]{0,1:T(8,128)} %fusion.8) | copy-start | bytes 5505028
  117.3 2.4 %copy-start.15 = (bf16[1,2048,448]{1,2,0:T(8,128)(2,1)S(1)}, bf16[1,2048,448]{1,2,0:T(8,128)(2,1)}, u32[]{:S(2)}) copy-start(bf16[1,2048,448]{1,2,0:T(8,128)(2,1)} %param.19) | copy-start | bytes 5505028
  124.3 46.9 %copy-start.5 = (bf16[2,256,256]{2,1,0:T(8,128)(2,1)S(1)}, bf16[2,256,256]{2,1,0:T(8,128)(2,1)}, u32[]{:S(2)}) copy-start(bf16[2,256,256]{2,1,0:T(8,128)(2,1)} %param.26) | copy-start | bytes 786436
  124.3 46.9 %copy-start.6 = (bf16[128,512]{1,0:T(8,128)(2,1)S(1)}, bf16[128,512]{1,0:T(8,128)(2,1)}, u32[]{:S(2)}) copy-start(bf16[128,512]{1,0:T(8,128)(2,1)} %param.22) | copy-start | bytes 393220
  171.1 0.7 copy-start.10
  171.1 0.7 copy-start.9
  171.2 1.5 copy-start.1
  175.4 23.5 %copy-start.4 = (bf16[2,256,256]{2,1,0:T(8,128)(2,1)S(1)}, bf16[2,256,256]{2,1,0:T(8,128)(2,1)}, u32[]{:S(2)}) copy-start(bf16[2,256,256]{2,1,0:T(8,128)(2,1)} %param.27) | copy-start | bytes 786436
  175.4 23.5 %copy-start.7 = (bf16[128,512]{1,0:T(8,128)(2,1)S(1)}, bf16[128,512]{1,0:T(8,128)(2,1)}, u32[]{:S(2)}) copy-start(bf16[128,512]{1,0:T(8,128)(2,1)} %param.22) | copy-start | bytes 393220
  196.2 3.1 %copy-start.2 = (f32[128,512]{1,0:T(8,128)S(1)}, f32[128,512]{1,0:T(8,128)}, u32[]{:S(2)}) copy-start(f32[128,512]{1,0:T(8,128)} %get-tuple-element.18) | copy-start | bytes 786436
  196.2 3.1 %copy-start.3 = (bf16[128,512]{1,0:T(8,128)(2,1)S(1)}, bf16[128,512]{1,0:T(8,128)(2,1)}, u32[]{:S(2)}) copy-start(bf16[128,512]{1,0:T(8,128)(2,1)} %h_ref.1) | copy-start | bytes 393220
